TPU v7x, 32 devices: a whole 2x2x4 slice. The times are simulated.
32 devices in a mesh: sp: 4 (over y, x), tp: 8 (over z, core).
Axes of the slice: x: 2, y: 2, z: 4, core: 2. Of those that a mesh axis runs over, the one named last changes fastest.
Arguments:
- queries: bfloat16 [3072, 16, 128], P('sp', 'tp'), may hold values from -240 to 240
- key_pairs: bfloat16 [3072, 16, 128], P('sp', 'tp'), may hold values from -11 to 11
- head_values: bfloat16 [3072, 16, 128], P('sp', 'tp'), may hold values from -6 to 6
- lambdas: float32 [16], P('tp'), may hold values from 0.3 to 0.8
- head_gain: float32 [128], replicated, may hold values from 0.1 to 1.9
- out_weight: bfloat16 [2048, 2048], replicated, may hold values from -0.125 to 0.125
- residual: bfloat16 [3072, 2048], P(('sp', 'tp')), may hold values from -6 to 6
- norm_gain: float32 [2048], replicated, may hold values from 0.1 to 1.9
- expert_ids: int32 [3072, 2], P(('sp', 'tp')), may hold values from 0 to 7, all different within a row; in each aligned block of 96 rows (0 to 95, 96 to 191, ...) at most 32 rows name the same one
- route_weights: float32 [3072, 2], P(('sp', 'tp')), may hold values from 0.2 to 1
- gate_weight: bfloat16 [8, 2048, 2048], P('sp', None, 'tp'), may hold values from -0.125 to 0.125
- up_weight: bfloat16 [8, 2048, 2048], P('sp', None, 'tp'), may hold values from -0.125 to 0.125
- down_weight: bfloat16 [8, 2048, 2048], P('sp', 'tp'), may hold values from -0.125 to 0.125
Outputs:
- merged: bfloat16 [3072, 2048], P(('sp', 'tp'))
Inputs may be any that keep to these rules, and one draw needn't show every extreme that they name: `expert_ids`: within the rows of one device each expert is named at most 32 times, and exactly 32 times in some device.
All inputs are finite; a program needn't handle non-finite values.
Results may differ from a plain program's by a relative error of at most 0.019.
Values may be sent and summed in bfloat16 or wider, within the bound.
A program may use at most 128 MiB of HBM per device.

v0:
```python
import functools
import math

import jax
import jax.numpy as jnp
from jax import lax
from jax.experimental import pallas as pl
from jax.experimental.pallas import tpu as pltpu
from jax.sharding import PartitionSpec as P

MESH = pl.DeviceIdType.MESH
LOG2E = 1.4426950408889634
CORES = 2
VMEM_BYTES = 67043328


def attend_kernel(
    n_sp,
    n_tp,
    scale,
    lam_ref,
    q_ref,
    kv_ref,
    gain_ref,
    meta_ref,
    base_ref,
    norm_ref,
    w_hbm,
    updated_ref,
    normed_ref,
    zmeta_ref,
    weight,
    gathered,
    kvbuf,
    acc,
    top,
    tot,
    att,
    kv_send,
    kv_recv,
    at_send,
    at_recv,
    me_send,
    me_recv,
    own_sem,
    w_sem,
):
    heads, tiles, wide, _ = q_ref.shape
    tile = wide // 2
    rows = base_ref.shape[0]
    n_z = n_tp // CORES
    c = lax.axis_index("sp")
    t = lax.axis_index("tp")
    load = pltpu.make_async_copy(w_hbm, weight, w_sem)
    load.start()
    barrier = pltpu.get_barrier_semaphore()
    for d in range(1, n_sp):
        pl.semaphore_signal(barrier, inc=1, device_id=((c + d) % n_sp, t), device_id_type=MESH)
    for d in range(1, n_tp):
        pl.semaphore_signal(barrier, inc=1, device_id=(c, (t + d) % n_tp), device_id_type=MESH)
    pl.semaphore_wait(barrier, n_sp + n_tp - 2)

    def kv_copy(d, h):
        return pltpu.make_async_remote_copy(
            src_ref=kv_ref.at[h],
            dst_ref=kvbuf.at[d - 1, h],
            send_sem=kv_send.at[d - 1, h],
            recv_sem=kv_recv.at[d - 1, h],
            device_id=((c + d) % n_sp, t),
            device_id_type=MESH,
        )

    def meta_copy(d):
        return pltpu.make_async_remote_copy(
            src_ref=meta_ref,
            dst_ref=zmeta_ref.at[d],
            send_sem=me_send.at[d],
            recv_sem=me_recv.at[d],
            device_id=(c, (t + CORES * d) % n_tp),
            device_id_type=MESH,
        )

    for d in range(1, n_sp):
        @pl.when(c + d < n_sp)
        def _():
            for h in range(heads):
                kv_copy(d, h).start()

    for d in range(1, n_z):
        meta_copy(d).start()
    zmeta_ref[0] = meta_ref[...]

    factor = scale * LOG2E

    def scores_of(h, i, keys):
        return (
            lax.dot_general(
                q_ref[h, i], keys, (((1,), (1,)), ((), ())), preferred_element_type=jnp.float32
            )
            * factor
        )

    for i in range(tiles):
        extent = (i + 1) * tile
        for h in range(heads):
            s = scores_of(h, i, kv_ref[h, 0, :extent])
            row = lax.rem(lax.broadcasted_iota(jnp.int32, (wide, extent), 0), tile) + i * tile
            col = lax.broadcasted_iota(jnp.int32, (wide, extent), 1)
            s = jnp.where(col <= row, s, -jnp.inf)
            high = jnp.max(s, axis=1, keepdims=True)
            p = jnp.exp2(s - high)
            top[h, i] = high
            tot[h, i] = jnp.sum(p, axis=1, keepdims=True)
            acc[h, i] = jnp.dot(
                p.astype(jnp.bfloat16), kv_ref[h, 1, :extent], preferred_element_type=jnp.float32
            )

    def span_step(step, carry):
        for h in range(heads):
            kv_copy(step, h).wait_recv()

        def tile_step(i, inner):
            for h in range(heads):
                s = scores_of(h, i, kvbuf[step - 1, h, 0])
                before = top[h, i]
                high = jnp.maximum(before, jnp.max(s, axis=1, keepdims=True))
                p = jnp.exp2(s - high)
                decay = jnp.exp2(before - high)
                top[h, i] = high
                tot[h, i] = tot[h, i] * decay + jnp.sum(p, axis=1, keepdims=True)
                acc[h, i] = acc[h, i] * decay + jnp.dot(
                    p.astype(jnp.bfloat16),
                    kvbuf[step - 1, h, 1],
                    preferred_element_type=jnp.float32,
                )
            return inner

        return lax.fori_loop(0, tiles, tile_step, carry)

    lax.fori_loop(1, c + 1, span_step, 0)

    for h in range(heads):
        width = acc.shape[3]
        for i in range(tiles):
            both = acc[h, i] / tot[h, i]
            mixed = both[:tile] - lam_ref[h] * both[tile:]
            mean = jnp.mean(mixed * mixed, axis=1, keepdims=True)
            normed = mixed * lax.rsqrt(mean + 1e-06) * gain_ref[...]
            att[i * tile : (i + 1) * tile, h * width : (h + 1) * width] = normed.astype(att.dtype)

    def att_copy(d):
        to = (t + d) % n_tp
        return pltpu.make_async_remote_copy(
            src_ref=att.at[pl.ds(pl.multiple_of(to * rows, rows), rows)],
            dst_ref=gathered.at[t],
            send_sem=at_send.at[d],
            recv_sem=at_recv.at[d],
            device_id=(c, to),
            device_id_type=MESH,
        )

    for d in range(1, n_tp):
        att_copy(d).start()
    own = pltpu.make_async_copy(
        att.at[pl.ds(pl.multiple_of(t * rows, rows), rows)], gathered.at[t], own_sem
    )
    own.start()
    own.wait()
    load.wait()
    span = att.shape[1]
    projected = jnp.zeros(base_ref.shape, jnp.float32)
    for d in range(n_tp):
        if d:
            att_copy(d).wait_recv()
        source = (t - d + n_tp) % n_tp
        projected = projected + jnp.dot(
            gathered[source],
            weight[pl.ds(pl.multiple_of(source * span, span), span), :],
            preferred_element_type=jnp.float32,
        )
    updated = (base_ref[...].astype(jnp.float32) + projected).astype(jnp.bfloat16)
    updated_ref[...] = updated
    widened = updated.astype(jnp.float32)
    mean = jnp.mean(widened * widened, axis=1, keepdims=True)
    normed_ref[...] = (widened * lax.rsqrt(mean + 1e-06) * norm_ref[...]).astype(jnp.bfloat16)
    for d in range(1, n_tp):
        att_copy(d).wait_send()
    for d in range(1, n_z):
        meta_copy(d).wait()
    for d in range(1, n_sp):
        @pl.when(c + d < n_sp)
        def _():
            for h in range(heads):
                kv_copy(d, h).wait_send()


def attend(queries, key_pairs, head_values, lambdas, head_gain, meta, residual, norm_gain, out_weight, n_sp, n_tp):
    tokens, heads, pair = queries.shape
    rows = residual.shape[0]
    width = head_values.shape[2]
    half = pair // 2
    tile = math.gcd(tokens, 256)
    tiles = tokens // tile
    first = (jnp.arange(pair) < half)[None, :]
    q = jnp.transpose(queries, (1, 0, 2)).reshape(heads, tiles, 1, tile, pair)
    sides = jnp.stack([first, ~first])
    q = jnp.where(sides, q, jnp.zeros((), q.dtype)).reshape(heads, tiles, 2 * tile, pair)
    kv = jnp.transpose(jnp.stack([key_pairs, head_values]), (2, 0, 1, 3))
    dma = pltpu.SemaphoreType.DMA
    vmem = pl.BlockSpec(memory_space=pltpu.VMEM)
    n_z = n_tp // CORES
    return pl.pallas_call(
        functools.partial(attend_kernel, n_sp, n_tp, half ** (-0.5)),
        out_shape=(
            jax.ShapeDtypeStruct(residual.shape, jnp.bfloat16),
            jax.ShapeDtypeStruct(residual.shape, jnp.bfloat16),
            jax.ShapeDtypeStruct((n_z,) + meta.shape, meta.dtype),
        ),
        in_specs=[pl.BlockSpec(memory_space=pltpu.SMEM)] + [vmem] * 6
        + [pl.BlockSpec(memory_space=pl.ANY)],
        out_specs=(vmem, vmem, vmem),
        scratch_shapes=[
            pltpu.VMEM(out_weight.shape, out_weight.dtype),
            pltpu.VMEM((n_tp, rows, heads * width), jnp.bfloat16),
            pltpu.VMEM((n_sp - 1,) + kv.shape, kv.dtype),
            pltpu.VMEM((heads, tiles, 2 * tile, width), jnp.float32),
            pltpu.VMEM((heads, tiles, 2 * tile, 1), jnp.float32),
            pltpu.VMEM((heads, tiles, 2 * tile, 1), jnp.float32),
            pltpu.VMEM((tokens, heads * width), jnp.bfloat16),
            dma((n_sp - 1, heads)),
            dma((n_sp - 1, heads)),
            dma((n_tp,)),
            dma((n_tp,)),
            dma((n_z,)),
            dma((n_z,)),
            dma,
            dma,
        ],
        compiler_params=pltpu.CompilerParams(
            collective_id=0, has_side_effects=True, vmem_limit_bytes=48 * 1024 * 1024
        ),
        name="attend",
    )(lambdas, q, kv, head_gain.reshape(1, -1), meta, residual, norm_gain.reshape(1, -1), out_weight)


def experts_kernel(
    n_sp,
    n_z,
    x_ref,
    meta_ref,
    base_ref,
    gate_hbm,
    up_hbm,
    down_hbm,
    out_ref,
    gate,
    up,
    down,
    zrows,
    pack,
    arrived,
    psend,
    own,
    precv,
    ret,
    zsend,
    zret,
    mine,
    w_sem,
    zs_send,
    zs_recv,
    ps_send,
    ps_recv,
    fw_send,
    fw_recv,
    pp_send,
    pp_recv,
    rt_send,
    rt_recv,
    zr_send,
    zr_recv,
):
    rows, model = x_ref.shape
    local, cap = pack.shape[2], pack.shape[3]
    slots = n_sp * local * cap
    c = lax.axis_index("sp")
    t = lax.axis_index("tp")
    n_tp = n_z * CORES
    core = t % CORES
    partner = (c, t + 1 - 2 * core)
    loads = [
        pltpu.make_async_copy(a, b, w_sem.at[i])
        for i, (a, b) in enumerate(((gate_hbm, gate), (up_hbm, up), (down_hbm, down)))
    ]
    for load in loads:
        load.start()

    def column(d):
        return ((c + d) % n_sp, t)

    def layer(d):
        return (c, (t + CORES * d) % n_tp)

    barrier = pltpu.get_barrier_semaphore()
    for d in range(1, n_sp):
        pl.semaphore_signal(barrier, inc=1, device_id=column(d), device_id_type=MESH)
    for d in range(1, n_z):
        pl.semaphore_signal(barrier, inc=1, device_id=layer(d), device_id_type=MESH)
    pl.semaphore_signal(barrier, inc=1, device_id=partner, device_id_type=MESH)
    pl.semaphore_wait(barrier, n_sp + n_z - 1)

    def remote(src, dst, send, recv, target):
        return pltpu.make_async_remote_copy(
            src_ref=src,
            dst_ref=dst,
            send_sem=send,
            recv_sem=recv,
            device_id=target,
            device_id_type=MESH,
        )

    def z_copy(d):
        return remote(x_ref, zrows.at[d - 1], zs_send.at[d], zs_recv.at[d], layer(d))

    def pack_copy(d, s):
        return remote(
            pack.at[s, d - 1], arrived.at[0, s, d], ps_send.at[d, s], ps_recv.at[d, s], column(d)
        )

    def share_copy(d, s):
        return remote(
            arrived.at[0, s, d], arrived.at[1, s, d], fw_send.at[d, s], fw_recv.at[d, s], partner
        )

    def pair_copy(s):
        return remote(psend.at[s], precv.at[s], pp_send.at[s], pp_recv.at[s], partner)

    def back_copy(d, s):
        return remote(
            own.at[s, d], ret.at[s, d], rt_send.at[d, s], rt_recv.at[d, s], column(n_sp - d)
        )

    def z_back(d):
        return remote(
            zsend.at[d], zret.at[d], zr_send.at[d], zr_recv.at[d], layer(n_z - d)
        )

    for d in range(1, n_z):
        z_copy(d).start()

    def route_hits(s, r):
        target = lax.broadcasted_iota(jnp.int32, (slots, rows), 0).astype(jnp.float32)
        return target == meta_ref[s, r : r + 1, :rows]

    def pack_rows(s):
        if s:
            z_copy(s).wait_recv()
        hits = route_hits(s, 0) | route_hits(s, 1)
        pick = jnp.where(hits, 1.0, 0.0).astype(jnp.bfloat16)
        source = x_ref[...] if s == 0 else zrows[s - 1]
        packed = (
            jnp.dot(pick, source, preferred_element_type=jnp.float32)
            .astype(jnp.bfloat16)
            .reshape(n_sp, local, cap, model)
        )
        for d in range(1, n_sp):
            pack[s, d - 1] = packed[d]
            pack_copy(d, s).start()
        arrived[0, s, 0] = packed[0]
        share_copy(0, s).start()

    def run_experts(s):
        for d in range(1, n_sp):
            pack_copy(d, s).wait_recv()
            share_copy(d, s).start()
        for d in range(n_sp):
            share_copy(d, s).wait_recv()

        def expert_step(e, carry):
            x = arrived[:, s, :, e].reshape(2 * n_sp * cap, model)
            gated = jnp.dot(x, gate[e], preferred_element_type=jnp.float32)
            lifted = jnp.dot(x, up[e], preferred_element_type=jnp.float32)
            inner = (gated / (1.0 + jnp.exp(-gated)) * lifted).astype(jnp.bfloat16)
            y = jnp.dot(inner, down[e], preferred_element_type=jnp.float32)
            y = y.astype(jnp.bfloat16).reshape(2, n_sp, cap, model)
            own[s, :, e] = y[0]
            psend[s, :, e] = y[1]
            return carry

        lax.fori_loop(0, local, expert_step, 0)
        pair_copy(s).start()

    def reduce_pair(s):
        pair_copy(s).wait_recv()
        for d in list(range(1, n_sp)) + [0]:
            total = own[s, d].astype(jnp.float32) + precv[s, d].astype(jnp.float32)
            total = total.astype(jnp.bfloat16)
            if d == 0:
                ret[s, 0] = total
            else:
                own[s, d] = total
                back_copy(d, s).start()

    def mix_rows(s):
        for d in range(1, n_sp):
            back_copy(d, s).wait_recv()
        mixing = jnp.where(route_hits(s, 0), meta_ref[s, 2:3, :rows], 0.0) + jnp.where(
            route_hits(s, 1), meta_ref[s, 3:4, :rows], 0.0
        )
        high = mixing.astype(jnp.bfloat16)
        low = (mixing - high.astype(jnp.float32)).astype(jnp.bfloat16)
        back = ret[s].reshape(slots, model)
        numbers = (((0,), (0,)), ((), ()))
        merged = lax.dot_general(
            high, back, numbers, preferred_element_type=jnp.float32
        ) + lax.dot_general(low, back, numbers, preferred_element_type=jnp.float32)
        if s:
            zsend[s] = merged.astype(jnp.bfloat16)
            z_back(s).start()
        else:
            mine[...] = merged

    pack_rows(0)
    for load in loads:
        load.wait()
    if n_z > 1:
        pack_rows(1)
    for s in range(n_z):
        run_experts(s)
        if s + 2 < n_z:
            pack_rows(s + 2)
        elif s + 2 - n_z < n_z - 2:
            mix_rows(s + 2 - n_z)
        reduce_pair(s)
    for s in range(max(0, n_z - 2), n_z):
        mix_rows(s)
    merged = mine[...]
    for s in range(1, n_z):
        z_back(s).wait_recv()
        merged = merged + zret[s].astype(jnp.float32)
    out_ref[...] = (base_ref[...].astype(jnp.float32) + merged).astype(jnp.bfloat16)

    for d in range(1, n_z):
        z_copy(d).wait_send()
        z_back(d).wait_send()
    for s in range(n_z):
        for d in range(n_sp):
            if d:
                pack_copy(d, s).wait_send()
                back_copy(d, s).wait_send()
            share_copy(d, s).wait_send()
        pair_copy(s).wait_send()


def experts(normed, zmeta, updated, gate_weight, up_weight, down_weight, n_sp, n_z, cap):
    rows, model = normed.shape
    local = gate_weight.shape[0]
    dma = pltpu.SemaphoreType.DMA
    vmem = pl.BlockSpec(memory_space=pltpu.VMEM)
    hbm = pl.BlockSpec(memory_space=pl.ANY)
    block = (local, cap, model)

    def buffer(*shape):
        return pltpu.VMEM(shape, jnp.bfloat16)

    return pl.pallas_call(
        functools.partial(experts_kernel, n_sp, n_z),
        out_shape=jax.ShapeDtypeStruct((rows, model), jnp.bfloat16),
        in_specs=[vmem] * 3 + [hbm] * 3,
        out_specs=vmem,
        scratch_shapes=[
            buffer(*gate_weight.shape),
            buffer(*up_weight.shape),
            buffer(*down_weight.shape),
            buffer(n_z - 1, rows, model),
            buffer(n_z, n_sp - 1, *block),
            buffer(2, n_z, n_sp, *block),
            buffer(n_z, n_sp, *block),
            buffer(n_z, n_sp, *block),
            buffer(n_z, n_sp, *block),
            buffer(n_z, n_sp, *block),
            buffer(n_z, rows, model),
            buffer(n_z, rows, model),
            pltpu.VMEM((rows, model), jnp.float32),
            dma((3,)),
            dma((n_z,)),
            dma((n_z,)),
            dma((n_sp, n_z)),
            dma((n_sp, n_z)),
            dma((n_sp, n_z)),
            dma((n_sp, n_z)),
            dma((n_z,)),
            dma((n_z,)),
            dma((n_sp, n_z)),
            dma((n_sp, n_z)),
            dma((n_z,)),
            dma((n_z,)),
        ],
        compiler_params=pltpu.CompilerParams(
            collective_id=1, has_side_effects=True, vmem_limit_bytes=VMEM_BYTES
        ),
        name="experts",
    )(normed, zmeta, updated, gate_weight, up_weight, down_weight)


def shards(
    queries,
    key_pairs,
    head_values,
    lambdas,
    head_gain,
    out_weight,
    residual,
    norm_gain,
    expert_ids,
    route_weights,
    gate_weight,
    up_weight,
    down_weight,
):
    tokens_here, heads_here, pair_width = queries.shape
    value_width = head_values.shape[2]
    rows_here = residual.shape[0]
    sp_count = lax.axis_size("sp")
    tp_count = lax.axis_size("tp")
    z_count = tp_count // CORES
    route_count = expert_ids.shape[1]
    local_experts = gate_weight.shape[0]
    expert_count = local_experts * sp_count
    capacity = max(2, 4 * rows_here * route_count // (3 * expert_count))
    flat_ids = expert_ids.reshape(-1)
    indicator = (flat_ids[:, None] == jnp.arange(expert_count, dtype=jnp.int32)[None, :]).astype(
        jnp.int32
    )
    ranking = jnp.sum(jnp.cumsum(indicator, axis=0) * indicator, axis=1) - 1
    turned = (flat_ids - lax.axis_index("sp") * local_experts) % expert_count
    near_slots = (turned * capacity + ranking).reshape(rows_here, route_count)
    slots = flat_ids * capacity + ranking
    meta = jnp.concatenate([near_slots.astype(jnp.float32), route_weights], axis=1).T
    meta = jnp.pad(meta, ((0, 8 - 2 * route_count), (0, -rows_here % 128)), constant_values=-1.0)
    updated, normed, zmeta = attend(
        queries,
        key_pairs,
        head_values,
        lambdas,
        head_gain,
        meta,
        residual,
        norm_gain,
        out_weight,
        sp_count,
        tp_count,
    )
    model_width = normed.shape[1]
    block_bytes = z_count * local_experts * capacity * model_width * 2
    if capacity % 16 == 0 and rows_here <= 128 and route_count == 2 and (
        (7 * sp_count - 1) * block_bytes <= 3 * VMEM_BYTES // 5
    ):
        return experts(
            normed, zmeta, updated, gate_weight, up_weight, down_weight, sp_count, z_count, capacity
        )
    sources = jnp.arange(rows_here * route_count, dtype=jnp.int32) // route_count
    outgoing = (
        jnp.zeros((expert_count * capacity, model_width), jnp.bfloat16)
        .at[slots]
        .set(normed[sources])
    )
    arrived = lax.all_to_all(
        outgoing.reshape(sp_count, local_experts, capacity, model_width),
        "sp",
        split_axis=0,
        concat_axis=0,
        tiled=True,
    )
    piece_rows = lax.all_gather(arrived[None], "tp", axis=0, tiled=True)
    gate_part = jnp.einsum(
        "tsecd,edf->tsecf", piece_rows, gate_weight, preferred_element_type=jnp.float32
    )
    up_part = jnp.einsum(
        "tsecd,edf->tsecf", piece_rows, up_weight, preferred_element_type=jnp.float32
    )
    inner_rows = (jax.nn.silu(gate_part) * up_part).astype(jnp.bfloat16)
    partial_value = jnp.einsum(
        "tsecf,efd->tsecd", inner_rows, down_weight, preferred_element_type=jnp.float32
    )
    reduced = lax.psum_scatter(
        partial_value.astype(jnp.bfloat16), "tp", scatter_dimension=0, tiled=True
    )
    returned = lax.all_to_all(reduced[0], "sp", split_axis=0, concat_axis=0, tiled=True)
    picked = (
        returned.reshape(expert_count * capacity, model_width)[slots]
        .astype(jnp.float32)
        .reshape(rows_here, route_count, model_width)
    )
    moe_sum = jnp.sum(picked * route_weights[:, :, None], axis=1)
    return (updated.astype(jnp.float32) + moe_sum).astype(jnp.bfloat16)


def solution(mesh):
    placed = (
        P("sp", "tp", None),
        P("sp", "tp", None),
        P("sp", "tp", None),
        P("tp"),
        P(),
        P(),
        P(("sp", "tp"), None),
        P(),
        P(("sp", "tp"), None),
        P(("sp", "tp"), None),
        P("sp", None, "tp"),
        P("sp", None, "tp"),
        P("sp", "tp", None),
    )
    return jax.shard_map(
        shards, mesh=mesh, in_specs=placed, out_specs=P(("sp", "tp"), None), check_vma=False
    )
```

profile of v0, /device:TPU:0, one launch (start us, length us, event | category | flops | bytes accessed | tf_op | source)
XLA Modules:
  0.0 191.1 jit_solution(5723656514383899226)
XLA Ops:
  0.0 0.8 copy.20
  0.9 0.1 eq.24
  1.0 0.6 reduce-window.6
  1.6 0.2 slice_reduce_fusion
  1.9 0.1 add_bitcast_fusion
  2.0 0.1 sub.16
  2.1 0.1 copy.21
  2.2 0.7 fusion.4
  2.9 0.7 maximum_bitcast_fusion.1
  3.6 1.1 copy.17
  4.7 0.0 copy-start
  4.7 0.0 copy-start.4
  4.7 0.0 copy-start.5
  4.7 0.0 copy-start.6
  4.7 0.1 bitcast_select_fusion.q_ref
  4.8 0.1 copy_bitcast_fusion
  4.9 0.1 maximum_bitcast_fusion.kv_ref
  5.0 0.7 copy-done
  5.7 40.3 %attend.1 = (bf16[96,2048]{1,0:T(8,128)(2,1)S(1)}, bf16[96,2048]{1,0:T(8,128)(2,1)S(1)}, f32[4,8,128]{2,1,0:T(8,128)S(1)}) custom-call(f32[2]{0:T(128)S(1)} %copy-done.5, bf16[2,3,512,128]{3,2,1,0:T(8,128)(2,1)S(1)} %bitcast_select_fusion.q_ref, bf16[2,2,768,128]{3,2,1,0:T(8,128)(2,1)S(1)} %maximum_bitcast_fusion.kv_ref, f32[1,128]{1,0:T(1,128)S(1)} %bitcast.25, ...), custom_call_target="tpu_custom_call" | custom-call | tf_op jit(solution)/shard_map/attend/pallas_call | solution.py:212
  46.0 0.7 copy-done.1
  46.7 0.7 copy-done.2
  47.5 0.6 copy-done.3
  48.1 141.3 %experts.1 = bf16[96,2048]{1,0:T(8,128)(2,1)} custom-call(bf16[96,2048]{1,0:T(8,128)(2,1)} %copy-done.2, f32[4,8,128]{2,1,0:T(8,128)} %copy-done.3, bf16[96,2048]{1,0:T(8,128)(2,1)} %copy-done.1, bf16[2,2048,256]{2,1,0:T(8,128)(2,1)} %gate_hbm.1, bf16[2,2048,256]{2,1,0:T(8,128)(2,1)} %up_hbm.1, bf16[2,256,2048]{2,1,0:T(8,128)(2,1)} %down_hbm.1), custom_call_target="tpu_custom_call" | custom-call | tf_op jit(solution)/shard_map/experts/pallas_call | solution.py:466
  189.4 1.8 copy.25
  (20 shorter events, 0.2 us)
Async XLA Ops:
  0.0 4.8 %copy-start.7 = (bf16[768,2,128]{2,1,0:T(2,128)(2,1)S(1)}, bf16[768,2,128]{2,1,0:T(2,128)(2,1)}, u32[]{:S(2)}) copy-start(bf16[768,2,128]{2,1,0:T(2,128)(2,1)} %param.15) | copy-start | bytes 1179652
  0.0 4.8 %copy-start.8 = (bf16[768,2,128]{2,1,0:T(2,128)(2,1)S(1)}, bf16[768,2,128]{2,1,0:T(2,128)(2,1)}, u32[]{:S(2)}) copy-start(bf16[768,2,128]{2,1,0:T(2,128)(2,1)} %param.14) | copy-start | bytes 1179652
  4.7 1.0 copy-start
  4.7 1.0 copy-start.4
  4.7 1.0 copy-start.5
  4.7 1.0 copy-start.6
  46.0 0.7 copy-start.1
  46.7 0.7 copy-start.2
  47.5 0.6 copy-start.3
where the time goes:
time: 192 us; the launch traced here: 191 us
  Pallas kernels  182 us (95%)
  local copies, waits for them, and re-layouts  7.11 us (4%)
  other arithmetic  2.3 us (1%)
    pallas_call x1, Pallas kernels, experts(): pl.pallas_call(functools.partial(experts_kernel, n_sp, n_z), out_shape=ja...  141 us
    pallas_call x1, Pallas kernels, attend(): pl.pallas_call(functools.partial(attend_kernel, n_sp, n_tp, half ** (-0.5...  40.3 us
    unnamed x20, local copies, waits for them, and re-layouts  5.37 us

commit v1 on v0

--- a/solution.py
+++ b/solution.py
@@ -11,6 +11,8 @@
 MESH = pl.DeviceIdType.MESH
 LOG2E = 1.4426950408889634
 CORES = 2
+PLANE = 4
+HEADS_HERE = 2
 VMEM_BYTES = 67043328
 
 
@@ -503,6 +505,544 @@
     )(normed, zmeta, updated, gate_weight, up_weight, down_weight)
 
 
+def layer_kernel(
+    n_sp,
+    n_tp,
+    scale,
+    lam_ref,
+    q_ref,
+    kv_ref,
+    gain_ref,
+    meta_ref,
+    base_ref,
+    norm_ref,
+    w_hbm,
+    gate_hbm,
+    up_hbm,
+    down_hbm,
+    out_ref,
+    weight,
+    gathered,
+    kvbuf,
+    acc,
+    top,
+    tot,
+    att,
+    updated,
+    x_ref,
+    zmeta,
+    gate,
+    up,
+    down,
+    zrows,
+    pack,
+    arrived,
+    psend,
+    own,
+    precv,
+    ret,
+    zsend,
+    zret,
+    mine,
+    kv_send,
+    kv_recv,
+    at_send,
+    at_recv,
+    me_send,
+    me_recv,
+    w_sem,
+    zs_send,
+    zs_recv,
+    ps_send,
+    ps_recv,
+    fw_send,
+    fw_recv,
+    pp_send,
+    pp_recv,
+    rt_send,
+    rt_recv,
+    zr_send,
+    zr_recv,
+    go,
+):
+    heads, tiles, wide, _ = q_ref.shape
+    tile = wide // 2
+    rows, model = base_ref.shape
+    width = kv_ref.shape[3]
+    n_z = n_tp // CORES
+    local, cap = pack.shape[2], pack.shape[3]
+    slots = n_sp * local * cap
+    c = lax.axis_index("sp")
+    t = lax.axis_index("tp")
+    core = t % CORES
+    partner = (c, t + 1 - 2 * core)
+
+    def column(d):
+        return ((c + d) % n_sp, t)
+
+    def layer(d):
+        return (c, (t + CORES * d) % n_tp)
+
+    loads = [
+        pltpu.make_async_copy(a, b, w_sem.at[i])
+        for i, (a, b) in enumerate(
+            [(w_hbm.at[:, h], weight.at[h]) for h in range(heads)]
+            + [(gate_hbm, gate), (up_hbm, up), (down_hbm, down)]
+        )
+    ]
+    for load in loads:
+        load.start()
+    barrier = pltpu.get_barrier_semaphore()
+    for d in range(1, n_sp):
+        pl.semaphore_signal(barrier, inc=1, device_id=column(d), device_id_type=MESH)
+    for d in range(1, n_tp):
+        pl.semaphore_signal(barrier, inc=1, device_id=(c, (t + d) % n_tp), device_id_type=MESH)
+    pl.semaphore_wait(barrier, n_sp + n_tp - 2)
+
+    def remote(src, dst, send, recv, target):
+        return pltpu.make_async_remote_copy(
+            src_ref=src,
+            dst_ref=dst,
+            send_sem=send,
+            recv_sem=recv,
+            device_id=target,
+            device_id_type=MESH,
+        )
+
+    def kv_copies(slot, source, h, to, mine_too, parts=(0, 1)):
+        return [
+            remote(
+                kv_ref.at[h, part] if mine_too else kvbuf.at[source, h, part],
+                kvbuf.at[source, h, part],
+                kv_send.at[slot, part],
+                kv_recv.at[source, h, part],
+                (to, t),
+            )
+            for part in parts
+        ]
+
+    def kv_wait(source, h):
+        for part in range(2):
+            remote(
+                kvbuf.at[source, h, part],
+                kvbuf.at[source, h, part],
+                kv_send.at[0, part],
+                kv_recv.at[source, h, part],
+                partner,
+            ).wait_recv()
+
+    first_sends = [
+        kv_copies(0, 0, 0, 2, True)
+        + kv_copies(1, 0, 1, 1, True)
+        + kv_copies(2, 0, 1, 2, True)
+        + kv_copies(3, 0, 0, 1, True),
+        kv_copies(0, 1, 0, 3, True) + kv_copies(1, 1, 1, 0, True) + kv_copies(2, 1, 1, 3, True),
+        kv_copies(0, 2, 0, 3, True) + kv_copies(1, 2, 1, 3, True, (0,)),
+        [],
+    ]
+    relayed = [(1, 1), (0, 1), (0, 0), (1, 0)]
+    late_sends = [
+        kv_copies(4, 1, 1, 2, False),
+        kv_copies(3, 0, 1, 3, False),
+        kv_copies(2, 0, 0, 3, False) + kv_copies(1, 2, 1, 3, True, (1,)),
+        kv_copies(0, 1, 0, 2, False),
+    ]
+
+    def meta_copy(d):
+        return remote(meta_ref, zmeta.at[d], me_send.at[d], me_recv.at[d], layer(d))
+
+    for k in range(n_sp):
+        @pl.when(c == k)
+        def _():
+            for copy in first_sends[k]:
+                copy.start()
+
+    for d in range(1, n_z):
+        meta_copy(d).start()
+    zmeta[0] = meta_ref[...]
+
+    factor = scale * LOG2E
+
+    def scores_of(h, i, keys):
+        return (
+            lax.dot_general(
+                q_ref[h, i], keys, (((1,), (1,)), ((), ())), preferred_element_type=jnp.float32
+            )
+            * factor
+        )
+
+    for i in range(tiles):
+        extent = (i + 1) * tile
+        for h in range(heads):
+            s = scores_of(h, i, kv_ref[h, 0, :extent])
+            row = lax.rem(lax.broadcasted_iota(jnp.int32, (wide, extent), 0), tile) + i * tile
+            col = lax.broadcasted_iota(jnp.int32, (wide, extent), 1)
+            s = jnp.where(col <= row, s, -jnp.inf)
+            high = jnp.max(s, axis=1, keepdims=True)
+            p = jnp.exp2(s - high)
+            top[h, i] = high
+            tot[h, i] = jnp.sum(p, axis=1, keepdims=True)
+            acc[h, i] = jnp.dot(
+                p.astype(jnp.bfloat16), kv_ref[h, 1, :extent], preferred_element_type=jnp.float32
+            )
+
+    for k in range(n_sp):
+        @pl.when(c == k)
+        def _():
+            kv_wait(*relayed[k])
+            for copy in late_sends[k]:
+                copy.start()
+
+    def order_of(orders):
+        codes = [sum((2 * s + h) * 8**j for j, (s, h) in enumerate(o)) for o in orders]
+        code, count = jnp.int32(codes[0]), jnp.int32(len(orders[0]))
+        for k in range(1, n_sp):
+            code = jnp.where(c == k, codes[k], code)
+            count = jnp.where(c == k, len(orders[k]), count)
+        return code, count
+
+    def absorb(orders, waited):
+        code, count = order_of(orders)
+
+        def piece_step(j, code):
+            piece = code % 8
+            source, h = piece // 2, piece % 2
+
+            @pl.when(j >= waited)
+            def _():
+                kv_wait(source, h)
+
+            def tile_step(i, inner):
+                s = scores_of(h, i, kvbuf[source, h, 0])
+                before = top[h, i]
+                high = jnp.maximum(before, jnp.max(s, axis=1, keepdims=True))
+                p = jnp.exp2(s - high)
+                decay = jnp.exp2(before - high)
+                top[h, i] = high
+                tot[h, i] = tot[h, i] * decay + jnp.sum(p, axis=1, keepdims=True)
+                acc[h, i] = acc[h, i] * decay + jnp.dot(
+                    p.astype(jnp.bfloat16),
+                    kvbuf[source, h, 1],
+                    preferred_element_type=jnp.float32,
+                )
+                return inner
+
+            lax.fori_loop(0, tiles, tile_step, 0)
+            return code // 8
+
+        lax.fori_loop(0, count, piece_step, code)
+
+    def att_copy(h, d):
+        to = (t + d) % n_tp
+        return remote(
+            att.at[h, pl.ds(pl.multiple_of(to * rows, rows), rows)],
+            gathered.at[h, :, pl.ds(pl.multiple_of(t * width, width), width)],
+            at_send.at[h, d],
+            at_recv.at[h, d],
+            (c, to),
+        )
+
+    def finish(h):
+        for i in range(tiles):
+            both = acc[h, i] / tot[h, i]
+            mixed = both[:tile] - lam_ref[h] * both[tile:]
+            mean = jnp.mean(mixed * mixed, axis=1, keepdims=True)
+            normed = mixed * lax.rsqrt(mean + 1e-06) * gain_ref[...]
+            att[h, i * tile : (i + 1) * tile] = normed.astype(att.dtype)
+        for d in range(1, n_tp):
+            att_copy(h, d).start()
+        gathered[h, :, pl.ds(pl.multiple_of(t * width, width), width)] = att[
+            h, pl.ds(pl.multiple_of(t * rows, rows), rows)
+        ]
+
+    def project(h):
+        loads[h].wait()
+        for d in range(1, n_tp):
+            att_copy(h, d).wait_recv()
+        return jnp.dot(
+            gathered[h],
+            weight[h].reshape(n_tp * width, model),
+            preferred_element_type=jnp.float32,
+        )
+
+    absorb([[], [(0, 1), (0, 0)], [(0, 0), (0, 1), (1, 0)], [(1, 0), (2, 0), (1, 1), (0, 0)]], 1)
+    finish(0)
+    absorb([[], [], [(1, 1)], [(2, 1), (0, 1)]], 0)
+
+    @pl.when(c == n_sp - 1)
+    def _():
+        for d in range(1, n_sp):
+            pl.semaphore_signal(go, inc=1, device_id=column(d), device_id_type=MESH)
+
+    finish(1)
+    mine[...] = project(0)
+    new = (base_ref[...].astype(jnp.float32) + mine[...] + project(1)).astype(jnp.bfloat16)
+    updated[...] = new
+    widened = new.astype(jnp.float32)
+    mean = jnp.mean(widened * widened, axis=1, keepdims=True)
+    x_ref[...] = (widened * lax.rsqrt(mean + 1e-06) * norm_ref[...]).astype(jnp.bfloat16)
+
+    def z_copy(d):
+        return remote(x_ref, zrows.at[d - 1], zs_send.at[d], zs_recv.at[d], layer(d))
+
+    def pack_copy(d, s):
+        return remote(
+            pack.at[s, d - 1], arrived.at[0, s, d], ps_send.at[d, s], ps_recv.at[d, s], column(d)
+        )
+
+    def share_copy(d, s):
+        return remote(
+            arrived.at[0, s, d], arrived.at[1, s, d], fw_send.at[d, s], fw_recv.at[d, s], partner
+        )
+
+    def pair_copy(s):
+        return remote(psend.at[s], precv.at[s], pp_send.at[s], pp_recv.at[s], partner)
+
+    def back_copy(d, s):
+        return remote(
+            own.at[s, d], ret.at[s, d], rt_send.at[d, s], rt_recv.at[d, s], column(n_sp - d)
+        )
+
+    def z_back(d):
+        return remote(zsend.at[d], zret.at[d], zr_send.at[d], zr_recv.at[d], layer(n_z - d))
+
+    for d in range(1, n_z):
+        z_copy(d).start()
+    for d in range(1, n_z):
+        meta_copy(d).wait()
+
+    def route_hits(s, r):
+        target = lax.broadcasted_iota(jnp.int32, (slots, rows), 0).astype(jnp.float32)
+        return target == zmeta[s, r : r + 1, :rows]
+
+    def pack_rows(s):
+        if s:
+            z_copy(s).wait_recv()
+        hits = route_hits(s, 0) | route_hits(s, 1)
+        pick = jnp.where(hits, 1.0, 0.0).astype(jnp.bfloat16)
+        source = x_ref[...] if s == 0 else zrows[s - 1]
+        packed = (
+            jnp.dot(pick, source, preferred_element_type=jnp.float32)
+            .astype(jnp.bfloat16)
+            .reshape(n_sp, local, cap, model)
+        )
+        for d in range(1, n_sp):
+            pack[s, d - 1] = packed[d]
+            pack_copy(d, s).start()
+        arrived[0, s, 0] = packed[0]
+        share_copy(0, s).start()
+
+    def run_experts(s):
+        for d in range(1, n_sp):
+            pack_copy(d, s).wait_recv()
+            share_copy(d, s).start()
+        for d in range(n_sp):
+            share_copy(d, s).wait_recv()
+
+        def expert_step(e, carry):
+            x = arrived[:, s, :, e].reshape(2 * n_sp * cap, model)
+            gated = jnp.dot(x, gate[e], preferred_element_type=jnp.float32)
+            lifted = jnp.dot(x, up[e], preferred_element_type=jnp.float32)
+            inner = (gated / (1.0 + jnp.exp(-gated)) * lifted).astype(jnp.bfloat16)
+            y = jnp.dot(inner, down[e], preferred_element_type=jnp.float32)
+            y = y.astype(jnp.bfloat16).reshape(2, n_sp, cap, model)
+            own[s, :, e] = y[0]
+            psend[s, :, e] = y[1]
+            return carry
+
+        lax.fori_loop(0, local, expert_step, 0)
+        pair_copy(s).start()
+
+    def reduce_pair(s):
+        pair_copy(s).wait_recv()
+        for d in list(range(1, n_sp)) + [0]:
+            total = own[s, d].astype(jnp.float32) + precv[s, d].astype(jnp.float32)
+            total = total.astype(jnp.bfloat16)
+            if d == 0:
+                ret[s, 0] = total
+            else:
+                own[s, d] = total
+                back_copy(d, s).start()
+
+    def mix_rows(s):
+        for d in range(1, n_sp):
+            back_copy(d, s).wait_recv()
+        mixing = jnp.where(route_hits(s, 0), zmeta[s, 2:3, :rows], 0.0) + jnp.where(
+            route_hits(s, 1), zmeta[s, 3:4, :rows], 0.0
+        )
+        high = mixing.astype(jnp.bfloat16)
+        low = (mixing - high.astype(jnp.float32)).astype(jnp.bfloat16)
+        back = ret[s].reshape(slots, model)
+        numbers = (((0,), (0,)), ((), ()))
+        merged = lax.dot_general(
+            high, back, numbers, preferred_element_type=jnp.float32
+        ) + lax.dot_general(low, back, numbers, preferred_element_type=jnp.float32)
+        if s:
+            zsend[s] = merged.astype(jnp.bfloat16)
+            z_back(s).start()
+        return merged
+
+    @pl.when(c != n_sp - 1)
+    def _():
+        pl.semaphore_wait(go, 1)
+
+    pack_rows(0)
+    for load in loads[heads:]:
+        load.wait()
+    for s in range(1, n_z):
+        pack_rows(s)
+        run_experts(s - 1)
+        if s > 1:
+            reduce_pair(s - 1)
+    run_experts(n_z - 1)
+    for s in range(1, n_z - 1):
+        mix_rows(s)
+    reduce_pair(n_z - 1)
+    reduce_pair(0)
+    mix_rows(n_z - 1)
+    merged = updated[...].astype(jnp.float32)
+    for s in range(1, n_z):
+        z_back(s).wait_recv()
+        merged = merged + zret[s].astype(jnp.float32)
+    mine[...] = merged
+    out_ref[...] = (mine[...] + mix_rows(0)).astype(jnp.bfloat16)
+
+    for k in range(n_sp):
+        @pl.when(c == k)
+        def _():
+            for copy in first_sends[k] + late_sends[k]:
+                copy.wait_send()
+
+    for d in range(1, n_tp):
+        for h in range(heads):
+            att_copy(h, d).wait_send()
+    for d in range(1, n_z):
+        z_copy(d).wait_send()
+        z_back(d).wait_send()
+    for s in range(n_z):
+        for d in range(n_sp):
+            if d:
+                pack_copy(d, s).wait_send()
+                back_copy(d, s).wait_send()
+            share_copy(d, s).wait_send()
+        pair_copy(s).wait_send()
+
+
+def masked_queries(queries, tile):
+    tokens, heads, pair = queries.shape
+    tiles = tokens // tile
+    first = (jnp.arange(pair) < pair // 2)[None, :]
+    q = jnp.transpose(queries, (1, 0, 2)).reshape(heads, tiles, 1, tile, pair)
+    sides = jnp.stack([first, ~first])
+    return jnp.where(sides, q, jnp.zeros((), q.dtype)).reshape(heads, tiles, 2 * tile, pair)
+
+
+def whole_layer(
+    queries,
+    key_pairs,
+    head_values,
+    lambdas,
+    head_gain,
+    meta,
+    residual,
+    norm_gain,
+    out_weight,
+    gate_weight,
+    up_weight,
+    down_weight,
+    n_sp,
+    n_tp,
+    cap,
+):
+    tokens, heads, pair = queries.shape
+    rows, model = residual.shape
+    width = head_values.shape[2]
+    local = gate_weight.shape[0]
+    n_z = n_tp // CORES
+    tile = math.gcd(tokens, 256)
+    tiles = tokens // tile
+    q = masked_queries(queries, tile)
+    kv = jnp.transpose(jnp.stack([key_pairs, head_values]), (2, 0, 1, 3))
+    dma = pltpu.SemaphoreType.DMA
+    vmem = pl.BlockSpec(memory_space=pltpu.VMEM)
+    hbm = pl.BlockSpec(memory_space=pl.ANY)
+    block = (local, cap, model)
+
+    def buffer(*shape):
+        return pltpu.VMEM(shape, jnp.bfloat16)
+
+    def single(*shape):
+        return pltpu.VMEM(shape, jnp.float32)
+
+    return pl.pallas_call(
+        functools.partial(layer_kernel, n_sp, n_tp, (pair // 2) ** (-0.5)),
+        out_shape=jax.ShapeDtypeStruct((rows, model), jnp.bfloat16),
+        in_specs=[pl.BlockSpec(memory_space=pltpu.SMEM)] + [vmem] * 6 + [hbm] * 4,
+        out_specs=vmem,
+        scratch_shapes=[
+            buffer(heads, n_tp, width, model),
+            buffer(heads, rows, n_tp * width),
+            buffer(n_sp - 1, *kv.shape),
+            single(heads, tiles, 2 * tile, width),
+            single(heads, tiles, 2 * tile, 1),
+            single(heads, tiles, 2 * tile, 1),
+            buffer(heads, tokens, width),
+            buffer(rows, model),
+            buffer(rows, model),
+            single(n_z, *meta.shape),
+            buffer(*gate_weight.shape),
+            buffer(*up_weight.shape),
+            buffer(*down_weight.shape),
+            buffer(n_z - 1, rows, model),
+            buffer(n_z, n_sp - 1, *block),
+            buffer(2, n_z, n_sp, *block),
+            buffer(n_z, n_sp, *block),
+            buffer(n_z, n_sp, *block),
+            buffer(n_z, n_sp, *block),
+            buffer(n_z, n_sp, *block),
+            buffer(n_z, rows, model),
+            buffer(n_z, rows, model),
+            single(rows, model),
+            dma((n_sp + 1, 2)),
+            dma((n_sp - 1, heads, 2)),
+            dma((heads, n_tp)),
+            dma((heads, n_tp)),
+            dma((n_z,)),
+            dma((n_z,)),
+            dma((heads + 3,)),
+            dma((n_z,)),
+            dma((n_z,)),
+            dma((n_sp, n_z)),
+            dma((n_sp, n_z)),
+            dma((n_sp, n_z)),
+            dma((n_sp, n_z)),
+            dma((n_z,)),
+            dma((n_z,)),
+            dma((n_sp, n_z)),
+            dma((n_sp, n_z)),
+            dma((n_z,)),
+            dma((n_z,)),
+            pltpu.SemaphoreType.REGULAR,
+        ],
+        compiler_params=pltpu.CompilerParams(
+            collective_id=2, has_side_effects=True, vmem_limit_bytes=VMEM_BYTES
+        ),
+        name="layer",
+    )(
+        lambdas,
+        q,
+        kv,
+        head_gain.reshape(1, -1),
+        meta,
+        residual,
+        norm_gain.reshape(1, -1),
+        out_weight.reshape(n_tp, heads, width, model),
+        gate_weight,
+        up_weight,
+        down_weight,
+    )
+
+
 def shards(
     queries,
     key_pairs,
@@ -538,6 +1078,29 @@
     slots = flat_ids * capacity + ranking
     meta = jnp.concatenate([near_slots.astype(jnp.float32), route_weights], axis=1).T
     meta = jnp.pad(meta, ((0, 8 - 2 * route_count), (0, -rows_here % 128)), constant_values=-1.0)
+    model_width = residual.shape[1]
+    block_bytes = z_count * local_experts * capacity * model_width * 2
+    if sp_count == PLANE and heads_here == HEADS_HERE and pair_width == value_width and (
+        capacity % 16 == 0 and rows_here <= 128 and route_count == 2
+        and (7 * sp_count - 1) * block_bytes <= 3 * VMEM_BYTES // 5
+    ):
+        return whole_layer(
+            queries,
+            key_pairs,
+            head_values,
+            lambdas,
+            head_gain,
+            meta,
+            residual,
+            norm_gain,
+            out_weight,
+            gate_weight,
+            up_weight,
+            down_weight,
+            sp_count,
+            tp_count,
+            capacity,
+        )
     updated, normed, zmeta = attend(
         queries,
         key_pairs,
@@ -551,8 +1114,6 @@
         sp_count,
         tp_count,
     )
-    model_width = normed.shape[1]
-    block_bytes = z_count * local_experts * capacity * model_width * 2
     if capacity % 16 == 0 and rows_here <= 128 and route_count == 2 and (
         (7 * sp_count - 1) * block_bytes <= 3 * VMEM_BYTES // 5
     ):

time: 192 us -> 177 us (0.922)
  Pallas kernels: 182 us -> 168 us
  local copies, waits for them, and re-layouts: 7.11 us -> 5.04 us
    pallas_call x2 -> x1, Pallas kernels: 182 us -> 168 us  [whole_layer(): pl.pallas_call(functools.partial(layer_kernel, n_sp, n_tp, (pair // 2) **...]
    unnamed x20 -> x4, local copies, waits for them, and re-layouts: 5.37 us -> 2.6 us
where the time goes in v1:
time: 177 us
  Pallas kernels  168 us (95%)
  local copies, waits for them, and re-layouts  5.04 us (3%)
  other arithmetic  4.08 us (2%)
    pallas_call x1, Pallas kernels, whole_layer(): pl.pallas_call(functools.partial(layer_kernel, n_sp, n_tp, (pair // 2) **...  168 us

profile of v1, /device:TPU:0, one launch (start us, length us, event | category | flops | bytes accessed | tf_op | source)
XLA Modules:
  0.0 177.0 jit_solution(6173209544275356851)
XLA Ops:
  0.0 0.0 copy-start
  0.0 0.8 copy.20
  0.8 0.1 eq.24
  1.0 0.6 reduce-window.6
  1.6 0.2 slice_reduce_fusion
  1.8 0.1 add_bitcast_fusion
  2.0 0.1 sub.16
  2.1 0.1 copy.21
  2.2 0.7 fusion.4
  2.9 0.7 maximum_bitcast_fusion.1
  3.6 0.6 pad.9.meta_ref
  4.2 1.2 copy_bitcast_fusion
  5.4 1.0 maximum_bitcast_fusion.kv_ref
  6.4 0.0 copy-done
  6.4 0.1 copy.17
  6.5 0.9 bitcast_select_fusion.q_ref
  7.4 167.8 %layer.1 = bf16[96,2048]{1,0:T(8,128)(2,1)} custom-call(f32[2]{0:T(128)} %lam_ref.1, bf16[2,3,512,128]{3,2,1,0:T(8,128)(2,1)} %bitcast_select_fusion.q_ref, bf16[2,2,768,128]{3,2,1,0:T(8,128)(2,1)} %maximum_bitcast_fusion.kv_ref, f32[1,128]{1,0:T(1,128)} %bitcast.29, f32[8,128]{1,0:T(8,128)} %pad.9.meta_ref, bf16[96,2048]{1,0:T(8,128)(2,1)} %base_ref.1, ...), custom_call_target="tpu_custom_call" | custom-call | tf_op jit(solution)/shard_map/layer/pallas_call | solution.py:977
  175.3 1.8 copy.25
  (9 shorter events, 0.1 us)
Async XLA Ops:
  0.0 6.4 %copy-start = (bf16[768,2,128]{2,1,0:T(2,128)(2,1)S(1)}, bf16[768,2,128]{2,1,0:T(2,128)(2,1)}, u32[]{:S(2)}) copy-start(bf16[768,2,128]{2,1,0:T(2,128)(2,1)} %param.13) | copy-start | bytes 1179652

commit v2 on v1

--- a/solution.py
+++ b/solution.py
@@ -13,6 +13,8 @@
 CORES = 2
 PLANE = 4
 HEADS_HERE = 2
+LAYERS = 4
+TWIN = 3
 VMEM_BYTES = 67043328
 
 
@@ -521,7 +523,6 @@
     up_hbm,
     down_hbm,
     out_ref,
-    weight,
     gathered,
     kvbuf,
     acc,
@@ -543,6 +544,7 @@
     ret,
     zsend,
     zret,
+    fold,
     mine,
     kv_send,
     kv_recv,
@@ -563,6 +565,10 @@
     rt_recv,
     zr_send,
     zr_recv,
+    tw_send,
+    tw_recv,
+    fo_send,
+    fo_recv,
     go,
 ):
     heads, tiles, wide, _ = q_ref.shape
@@ -572,6 +578,7 @@
     n_z = n_tp // CORES
     local, cap = pack.shape[2], pack.shape[3]
     slots = n_sp * local * cap
+    span = n_sp * local * cap
     c = lax.axis_index("sp")
     t = lax.axis_index("tp")
     core = t % CORES
@@ -580,13 +587,21 @@
     def column(d):
         return ((c + d) % n_sp, t)
 
-    def layer(d):
-        return (c, (t + CORES * d) % n_tp)
-
+    z = t // CORES
+    twin_z = z + 1 - 2 * (z % 2)
+    far_z = (z + n_z // 2) % n_z
+    twin = (c, twin_z * CORES + core)
+    far = [None, (c, far_z * CORES + core), (c, (far_z + 1 - 2 * (far_z % 2)) * CORES + core)]
+
+    weight = (psend, precv)
     loads = [
         pltpu.make_async_copy(a, b, w_sem.at[i])
         for i, (a, b) in enumerate(
-            [(w_hbm.at[:, h], weight.at[h]) for h in range(heads)]
+            [
+                (w_hbm.at[source, h], weight[h].at[source * width : (source + 1) * width])
+                for h in range(heads)
+                for source in range(n_tp)
+            ]
             + [(gate_hbm, gate), (up_hbm, up), (down_hbm, down)]
         )
     ]
@@ -649,7 +664,7 @@
     ]
 
     def meta_copy(d):
-        return remote(meta_ref, zmeta.at[d], me_send.at[d], me_recv.at[d], layer(d))
+        return remote(meta_ref, zmeta.at[d], me_send.at[d], me_recv.at[d], far[d])
 
     for k in range(n_sp):
         @pl.when(c == k)
@@ -657,7 +672,7 @@
             for copy in first_sends[k]:
                 copy.start()
 
-    for d in range(1, n_z):
+    for d in (1, 2):
         meta_copy(d).start()
     zmeta[0] = meta_ref[...]
 
@@ -712,22 +727,21 @@
             def _():
                 kv_wait(source, h)
 
-            def tile_step(i, inner):
-                s = scores_of(h, i, kvbuf[source, h, 0])
+            keys, values = kvbuf[source, h, 0], kvbuf[source, h, 1]
+            results = []
+            for i in range(tiles):
+                s = scores_of(h, i, keys)
                 before = top[h, i]
                 high = jnp.maximum(before, jnp.max(s, axis=1, keepdims=True))
                 p = jnp.exp2(s - high)
                 decay = jnp.exp2(before - high)
-                top[h, i] = high
-                tot[h, i] = tot[h, i] * decay + jnp.sum(p, axis=1, keepdims=True)
-                acc[h, i] = acc[h, i] * decay + jnp.dot(
-                    p.astype(jnp.bfloat16),
-                    kvbuf[source, h, 1],
-                    preferred_element_type=jnp.float32,
+                total = tot[h, i] * decay + jnp.sum(p, axis=1, keepdims=True)
+                summed = acc[h, i] * decay + jnp.dot(
+                    p.astype(jnp.bfloat16), values, preferred_element_type=jnp.float32
                 )
-                return inner
-
-            lax.fori_loop(0, tiles, tile_step, 0)
+                results.append((high, total, summed))
+            for i in range(tiles):
+                top[h, i], tot[h, i], acc[h, i] = results[i]
             return code // 8
 
         lax.fori_loop(0, count, piece_step, code)
@@ -756,12 +770,13 @@
         ]
 
     def project(h):
-        loads[h].wait()
+        for load in loads[h * n_tp : (h + 1) * n_tp]:
+            load.wait()
         for d in range(1, n_tp):
             att_copy(h, d).wait_recv()
         return jnp.dot(
             gathered[h],
-            weight[h].reshape(n_tp * width, model),
+            weight[h][: n_tp * width],
             preferred_element_type=jnp.float32,
         )
 
@@ -783,7 +798,9 @@
     x_ref[...] = (widened * lax.rsqrt(mean + 1e-06) * norm_ref[...]).astype(jnp.bfloat16)
 
     def z_copy(d):
-        return remote(x_ref, zrows.at[d - 1], zs_send.at[d], zs_recv.at[d], layer(d))
+        if d == 1:
+            return remote(x_ref, zrows.at[0], zs_send.at[1], zs_recv.at[1], far[1])
+        return remote(zrows.at[0], zrows.at[1], zs_send.at[2], zs_recv.at[2], twin)
 
     def pack_copy(d, s):
         return remote(
@@ -795,8 +812,17 @@
             arrived.at[0, s, d], arrived.at[1, s, d], fw_send.at[d, s], fw_recv.at[d, s], partner
         )
 
+    def twin_copy(d):
+        return remote(
+            arrived.at[0, 0, d], arrived.at[0, TWIN, d], tw_send.at[d], tw_recv.at[d], twin
+        )
+
     def pair_copy(s):
-        return remote(psend.at[s], precv.at[s], pp_send.at[s], pp_recv.at[s], partner)
+        block = pl.ds(s * span, span)
+        return remote(psend.at[block], precv.at[block], pp_send.at[s], pp_recv.at[s], partner)
+
+    def fold_copy(d):
+        return remote(own.at[TWIN, d], fold.at[d], fo_send.at[d], fo_recv.at[d], twin)
 
     def back_copy(d, s):
         return remote(
@@ -804,11 +830,15 @@
         )
 
     def z_back(d):
-        return remote(zsend.at[d], zret.at[d], zr_send.at[d], zr_recv.at[d], layer(n_z - d))
-
-    for d in range(1, n_z):
-        z_copy(d).start()
-    for d in range(1, n_z):
+        return remote(zsend.at[d - 1], zret.at[d - 1], zr_send.at[d], zr_recv.at[d], far[d])
+
+    outer = (z == 0) | (z == n_z - 1)
+
+    @pl.when(jnp.logical_not(outer))
+    def _():
+        z_copy(1).start()
+
+    for d in (1, 2):
         meta_copy(d).wait()
 
     def route_hits(s, r):
@@ -818,6 +848,10 @@
     def pack_rows(s):
         if s:
             z_copy(s).wait_recv()
+        if s == 1:
+            z_copy(2).start()
+            for d in range(2, n_sp):
+                twin_copy(d).start()
         hits = route_hits(s, 0) | route_hits(s, 1)
         pick = jnp.where(hits, 1.0, 0.0).astype(jnp.bfloat16)
         source = x_ref[...] if s == 0 else zrows[s - 1]
@@ -826,18 +860,36 @@
             .astype(jnp.bfloat16)
             .reshape(n_sp, local, cap, model)
         )
+        if s == 0:
+            arrived[0, 0, 0] = packed[0]
+            twin_copy(0).start()
+
+            @pl.when(outer)
+            def _():
+                z_copy(1).start()
+
         for d in range(1, n_sp):
             pack[s, d - 1] = packed[d]
             pack_copy(d, s).start()
-        arrived[0, s, 0] = packed[0]
+        if s:
+            arrived[0, s, 0] = packed[0]
         share_copy(0, s).start()
 
-    def run_experts(s):
-        for d in range(1, n_sp):
-            pack_copy(d, s).wait_recv()
-            share_copy(d, s).start()
+    def rows_here(s):
+        for d in range(n_sp):
+            if s == TWIN:
+                twin_copy(d).wait_recv()
+            elif d:
+                pack_copy(d, s).wait_recv()
+            if s == 0 and d == 1:
+                twin_copy(d).start()
+            if s == TWIN or d:
+                share_copy(d, s).start()
         for d in range(n_sp):
             share_copy(d, s).wait_recv()
+
+    def run_experts(s):
+        rows_here(s)
 
         def expert_step(e, carry):
             x = arrived[:, s, :, e].reshape(2 * n_sp * cap, model)
@@ -847,7 +899,9 @@
             y = jnp.dot(inner, down[e], preferred_element_type=jnp.float32)
             y = y.astype(jnp.bfloat16).reshape(2, n_sp, cap, model)
             own[s, :, e] = y[0]
-            psend[s, :, e] = y[1]
+            for d in range(n_sp):
+                place = pl.multiple_of(s * span + (d * local + e) * cap, cap)
+                psend[pl.ds(place, cap)] = y[1, d]
             return carry
 
         lax.fori_loop(0, local, expert_step, 0)
@@ -856,9 +910,18 @@
     def reduce_pair(s):
         pair_copy(s).wait_recv()
         for d in list(range(1, n_sp)) + [0]:
-            total = own[s, d].astype(jnp.float32) + precv[s, d].astype(jnp.float32)
+            other = precv[s * span + d * local * cap : s * span + (d + 1) * local * cap]
+            total = own[s, d].astype(jnp.float32) + other.reshape(local, cap, model).astype(
+                jnp.float32
+            )
+            if s == 0:
+                fold_copy(d).wait_recv()
+                total = total + fold[d].astype(jnp.float32)
             total = total.astype(jnp.bfloat16)
-            if d == 0:
+            if s == TWIN:
+                own[s, d] = total
+                fold_copy(d).start()
+            elif d == 0:
                 ret[s, 0] = total
             else:
                 own[s, d] = total
@@ -878,7 +941,7 @@
             high, back, numbers, preferred_element_type=jnp.float32
         ) + lax.dot_general(low, back, numbers, preferred_element_type=jnp.float32)
         if s:
-            zsend[s] = merged.astype(jnp.bfloat16)
+            zsend[s - 1] = merged.astype(jnp.bfloat16)
             z_back(s).start()
         return merged
 
@@ -887,23 +950,24 @@
         pl.semaphore_wait(go, 1)
 
     pack_rows(0)
-    for load in loads[heads:]:
+    for load in loads[heads * n_tp :]:
         load.wait()
-    for s in range(1, n_z):
-        pack_rows(s)
-        run_experts(s - 1)
-        if s > 1:
-            reduce_pair(s - 1)
-    run_experts(n_z - 1)
-    for s in range(1, n_z - 1):
-        mix_rows(s)
-    reduce_pair(n_z - 1)
+    run_experts(0)
+    pack_rows(1)
+    pack_rows(2)
+    run_experts(1)
+    reduce_pair(1)
+    run_experts(TWIN)
+    reduce_pair(TWIN)
+    run_experts(2)
+    reduce_pair(2)
+    mix_rows(1)
+    mix_rows(2)
     reduce_pair(0)
-    mix_rows(n_z - 1)
     merged = updated[...].astype(jnp.float32)
-    for s in range(1, n_z):
+    for s in (1, 2):
         z_back(s).wait_recv()
-        merged = merged + zret[s].astype(jnp.float32)
+        merged = merged + zret[s - 1].astype(jnp.float32)
     mine[...] = merged
     out_ref[...] = (mine[...] + mix_rows(0)).astype(jnp.bfloat16)
 
@@ -916,16 +980,19 @@
     for d in range(1, n_tp):
         for h in range(heads):
             att_copy(h, d).wait_send()
-    for d in range(1, n_z):
+    for d in (1, 2):
         z_copy(d).wait_send()
         z_back(d).wait_send()
     for s in range(n_z):
         for d in range(n_sp):
-            if d:
+            if d and s != TWIN:
                 pack_copy(d, s).wait_send()
                 back_copy(d, s).wait_send()
             share_copy(d, s).wait_send()
         pair_copy(s).wait_send()
+    for d in range(n_sp):
+        twin_copy(d).wait_send()
+        fold_copy(d).wait_send()
 
 
 def masked_queries(queries, tile):
@@ -967,6 +1034,7 @@
     vmem = pl.BlockSpec(memory_space=pltpu.VMEM)
     hbm = pl.BlockSpec(memory_space=pl.ANY)
     block = (local, cap, model)
+    flat = max(n_tp * width, n_z * n_sp * local * cap)
 
     def buffer(*shape):
         return pltpu.VMEM(shape, jnp.bfloat16)
@@ -980,7 +1048,6 @@
         in_specs=[pl.BlockSpec(memory_space=pltpu.SMEM)] + [vmem] * 6 + [hbm] * 4,
         out_specs=vmem,
         scratch_shapes=[
-            buffer(heads, n_tp, width, model),
             buffer(heads, rows, n_tp * width),
             buffer(n_sp - 1, *kv.shape),
             single(heads, tiles, 2 * tile, width),
@@ -989,19 +1056,20 @@
             buffer(heads, tokens, width),
             buffer(rows, model),
             buffer(rows, model),
-            single(n_z, *meta.shape),
+            single(3, *meta.shape),
             buffer(*gate_weight.shape),
             buffer(*up_weight.shape),
             buffer(*down_weight.shape),
-            buffer(n_z - 1, rows, model),
-            buffer(n_z, n_sp - 1, *block),
+            buffer(2, rows, model),
+            buffer(3, n_sp - 1, *block),
             buffer(2, n_z, n_sp, *block),
+            buffer(flat, model),
             buffer(n_z, n_sp, *block),
-            buffer(n_z, n_sp, *block),
-            buffer(n_z, n_sp, *block),
-            buffer(n_z, n_sp, *block),
-            buffer(n_z, rows, model),
-            buffer(n_z, rows, model),
+            buffer(flat, model),
+            buffer(3, n_sp, *block),
+            buffer(2, rows, model),
+            buffer(2, rows, model),
+            buffer(n_sp, *block),
             single(rows, model),
             dma((n_sp + 1, 2)),
             dma((n_sp - 1, heads, 2)),
@@ -1009,7 +1077,7 @@
             dma((heads, n_tp)),
             dma((n_z,)),
             dma((n_z,)),
-            dma((heads + 3,)),
+            dma((heads * n_tp + 3,)),
             dma((n_z,)),
             dma((n_z,)),
             dma((n_sp, n_z)),
@@ -1022,6 +1090,10 @@
             dma((n_sp, n_z)),
             dma((n_z,)),
             dma((n_z,)),
+            dma((n_sp,)),
+            dma((n_sp,)),
+            dma((n_sp,)),
+            dma((n_sp,)),
             pltpu.SemaphoreType.REGULAR,
         ],
         compiler_params=pltpu.CompilerParams(
@@ -1080,7 +1152,7 @@
     meta = jnp.pad(meta, ((0, 8 - 2 * route_count), (0, -rows_here % 128)), constant_values=-1.0)
     model_width = residual.shape[1]
     block_bytes = z_count * local_experts * capacity * model_width * 2
-    if sp_count == PLANE and heads_here == HEADS_HERE and pair_width == value_width and (
+    if sp_count == PLANE and z_count == LAYERS and heads_here == HEADS_HERE and pair_width == value_width and (
         capacity % 16 == 0 and rows_here <= 128 and route_count == 2
         and (7 * sp_count - 1) * block_bytes <= 3 * VMEM_BYTES // 5
     ):

time: 177 us -> 153 us (0.86)
  the two profiles are of different devices: /device:TPU:0 before, /device:TPU:8 now
where the time goes in v2:
time: 153 us
  Pallas kernels  144 us (94%)
  local copies, waits for them, and re-layouts  5.04 us (3%)
  other arithmetic  4.08 us (3%)
    pallas_call x1, Pallas kernels, whole_layer(): pl.pallas_call(functools.partial(layer_kernel, n_sp, n_tp, (pair // 2) **...  144 us

profile of v2, /device:TPU:8, one launch (start us, length us, event | category | flops | bytes accessed | tf_op | source)
XLA Modules:
  0.0 153.2 jit_solution(4519586424478055619)
XLA Ops:
  0.0 0.0 copy-start
  0.0 0.8 copy.20
  0.8 0.1 eq.24
  1.0 0.6 reduce-window.6
  1.6 0.2 slice_reduce_fusion
  1.8 0.1 add_bitcast_fusion
  2.0 0.1 sub.16
  2.1 0.1 copy.21
  2.2 0.7 fusion.4
  2.9 0.7 maximum_bitcast_fusion.1
  3.6 0.6 pad.9.meta_ref
  4.2 1.2 copy_bitcast_fusion
  5.4 1.0 maximum_bitcast_fusion.kv_ref
  6.4 0.0 copy-done
  6.4 0.1 copy.17
  6.5 0.9 bitcast_select_fusion.q_ref
  7.4 144.0 %layer.1 = bf16[96,2048]{1,0:T(8,128)(2,1)} custom-call(f32[2]{0:T(128)} %lam_ref.1, bf16[2,3,512,128]{3,2,1,0:T(8,128)(2,1)} %bitcast_select_fusion.q_ref, bf16[2,2,768,128]{3,2,1,0:T(8,128)(2,1)} %maximum_bitcast_fusion.kv_ref, f32[1,128]{1,0:T(1,128)} %bitcast.29, f32[8,128]{1,0:T(8,128)} %pad.9.meta_ref, bf16[96,2048]{1,0:T(8,128)(2,1)} %base_ref.1, ...), custom_call_target="tpu_custom_call" | custom-call | tf_op jit(solution)/shard_map/layer/pallas_call | solution.py:1045
  151.5 1.8 %copy.25 = bf16[96,2048]{1,0:T(8,128)(2,1)} copy(bf16[96,2048]{1,0:T(8,128)(2,1)} %layer.1) | data formatting | bytes 786432
  (9 shorter events, 0.1 us)
Async XLA Ops:
  0.0 6.4 %copy-start = (bf16[768,2,128]{2,1,0:T(2,128)(2,1)S(1)}, bf16[768,2,128]{2,1,0:T(2,128)(2,1)}, u32[]{:S(2)}) copy-start(bf16[768,2,128]{2,1,0:T(2,128)(2,1)} %param.13) | copy-start | bytes 1179652

commit v3 on v2

--- a/solution.py
+++ b/solution.py
@@ -512,10 +512,12 @@
     n_tp,
     scale,
     lam_ref,
-    q_ref,
-    kv_ref,
+    raw_ref,
+    k_ref,
+    v_ref,
     gain_ref,
-    meta_ref,
+    ids_ref,
+    mix_ref,
     base_ref,
     norm_ref,
     w_hbm,
@@ -523,12 +525,14 @@
     up_hbm,
     down_hbm,
     out_ref,
+    q_ref,
     gathered,
     kvbuf,
     acc,
     top,
     tot,
     att,
+    bases,
     updated,
     x_ref,
     zmeta,
@@ -545,16 +549,18 @@
     zsend,
     zret,
     fold,
-    mine,
+    parts,
     kv_send,
     kv_recv,
     at_send,
     at_recv,
+    ar_send,
+    ar_recv,
+    ba_send,
+    ba_recv,
     me_send,
     me_recv,
     w_sem,
-    zs_send,
-    zs_recv,
     ps_send,
     ps_recv,
     fw_send,
@@ -574,7 +580,7 @@
     heads, tiles, wide, _ = q_ref.shape
     tile = wide // 2
     rows, model = base_ref.shape
-    width = kv_ref.shape[3]
+    width = v_ref.shape[2]
     n_z = n_tp // CORES
     local, cap = pack.shape[2], pack.shape[3]
     slots = n_sp * local * cap
@@ -627,7 +633,7 @@
     def kv_copies(slot, source, h, to, mine_too, parts=(0, 1)):
         return [
             remote(
-                kv_ref.at[h, part] if mine_too else kvbuf.at[source, h, part],
+                (k_ref, v_ref)[part].at[h] if mine_too else kvbuf.at[source, h, part],
                 kvbuf.at[source, h, part],
                 kv_send.at[slot, part],
                 kv_recv.at[source, h, part],
@@ -664,7 +670,7 @@
     ]
 
     def meta_copy(d):
-        return remote(meta_ref, zmeta.at[d], me_send.at[d], me_recv.at[d], far[d])
+        return remote(zmeta.at[0], zmeta.at[d], me_send.at[d], me_recv.at[d], far[d])
 
     for k in range(n_sp):
         @pl.when(c == k)
@@ -672,9 +678,50 @@
             for copy in first_sends[k]:
                 copy.start()
 
+    def base_copy(d, side):
+        columns = slice(side * (model // 2), (side + 1) * (model // 2))
+        return remote(
+            base_ref.at[:, columns] if d == 1 else bases.at[0, :, columns],
+            bases.at[d - 1, :, columns],
+            ba_send.at[d - 1, side],
+            ba_recv.at[d - 1, side],
+            far[1] if d == 1 else twin,
+        )
+
+    def pass_base(side):
+        base_copy(1, side).wait_recv()
+        base_copy(2, side).start()
+
+    for side in range(2):
+        base_copy(1, side).start()
+
+    experts = n_sp * local
+    shape = (experts, rows)
+    names = lax.broadcasted_iota(jnp.int32, shape, 0)
+    named = [names == ids_ref[r : r + 1, :] for r in range(2)]
+    chosen = jnp.where(named[0] | named[1], 1.0, 0.0).astype(jnp.bfloat16)
+    earlier = lax.broadcasted_iota(jnp.int32, (rows, rows), 0) < lax.broadcasted_iota(
+        jnp.int32, (rows, rows), 1
+    )
+    ranks = jnp.dot(
+        chosen, jnp.where(earlier, 1.0, 0.0).astype(jnp.bfloat16), preferred_element_type=jnp.float32
+    )
+    zmeta[0] = jnp.full(zmeta.shape[1:], -1.0, jnp.float32)
+    for r in range(2):
+        turned = ids_ref[r : r + 1, :] - c * local
+        turned = jnp.where(turned < 0, turned + experts, turned)
+        rank = jnp.sum(jnp.where(named[r], ranks, 0.0), axis=0, keepdims=True)
+        zmeta[0, r : r + 1, :rows] = (turned * cap).astype(jnp.float32) + rank
+        zmeta[0, 2 + r : 3 + r, :rows] = mix_ref[r : r + 1, :]
     for d in (1, 2):
         meta_copy(d).start()
-    zmeta[0] = meta_ref[...]
+
+    side = lax.broadcasted_iota(jnp.int32, (tile, raw_ref.shape[2]), 1) < raw_ref.shape[2] // 2
+    for h in range(heads):
+        for i in range(tiles):
+            part = raw_ref[h, i * tile : (i + 1) * tile]
+            q_ref[h, i, :tile] = jnp.where(side, part, jnp.zeros_like(part))
+            q_ref[h, i, tile:] = jnp.where(side, jnp.zeros_like(part), part)
 
     factor = scale * LOG2E
 
@@ -689,7 +736,7 @@
     for i in range(tiles):
         extent = (i + 1) * tile
         for h in range(heads):
-            s = scores_of(h, i, kv_ref[h, 0, :extent])
+            s = scores_of(h, i, k_ref[h, :extent])
             row = lax.rem(lax.broadcasted_iota(jnp.int32, (wide, extent), 0), tile) + i * tile
             col = lax.broadcasted_iota(jnp.int32, (wide, extent), 1)
             s = jnp.where(col <= row, s, -jnp.inf)
@@ -698,7 +745,7 @@
             top[h, i] = high
             tot[h, i] = jnp.sum(p, axis=1, keepdims=True)
             acc[h, i] = jnp.dot(
-                p.astype(jnp.bfloat16), kv_ref[h, 1, :extent], preferred_element_type=jnp.float32
+                p.astype(jnp.bfloat16), v_ref[h, :extent], preferred_element_type=jnp.float32
             )
 
     for k in range(n_sp):
@@ -707,6 +754,8 @@
             kv_wait(*relayed[k])
             for copy in late_sends[k]:
                 copy.start()
+
+    pass_base(0)
 
     def order_of(orders):
         codes = [sum((2 * s + h) * 8**j for j, (s, h) in enumerate(o)) for o in orders]
@@ -716,7 +765,7 @@
             count = jnp.where(c == k, len(orders[k]), count)
         return code, count
 
-    def absorb(orders, waited):
+    def absorb(orders, waited, passing=False):
         code, count = order_of(orders)
 
         def piece_step(j, code):
@@ -726,6 +775,12 @@
             @pl.when(j >= waited)
             def _():
                 kv_wait(source, h)
+
+            if passing:
+
+                @pl.when(j == count - 1)
+                def _():
+                    pass_base(1)
 
             keys, values = kvbuf[source, h, 0], kvbuf[source, h, 1]
             results = []
@@ -746,15 +801,39 @@
 
         lax.fori_loop(0, count, piece_step, code)
 
-    def att_copy(h, d):
+    half = n_z // 2
+
+    def block_rows(b, to_z, to_core):
+        layer = to_z if b == 0 else (to_z + half) % n_z
+        if b == 2:
+            layer = layer + 1 - 2 * (layer % 2)
+        return pl.ds(pl.multiple_of((layer * CORES + to_core) * rows, rows), rows)
+
+    here = pl.ds(pl.multiple_of(t * width, width), width)
+
+    def att_copy(h, b, d):
         to = (t + d) % n_tp
         return remote(
-            att.at[h, pl.ds(pl.multiple_of(to * rows, rows), rows)],
-            gathered.at[h, :, pl.ds(pl.multiple_of(t * width, width), width)],
-            at_send.at[h, d],
-            at_recv.at[h, d],
+            att.at[h, block_rows(b, to // CORES, to % CORES)],
+            gathered.at[h, b, :, here],
+            at_send.at[h, b, d],
+            at_recv.at[h, b, d],
             (c, to),
         )
+
+    def relay_copy(h):
+        side = half * CORES * width
+        across = pl.ds(pl.multiple_of((1 - z // half) * side, side), side)
+        return remote(
+            gathered.at[h, 1, :, across],
+            gathered.at[h, 2, :, across],
+            ar_send.at[h],
+            ar_recv.at[h],
+            twin,
+        )
+
+    def near(d):
+        return ((t + d) % n_tp) // CORES // half == z // half
 
     def finish(h):
         for i in range(tiles):
@@ -763,24 +842,58 @@
             mean = jnp.mean(mixed * mixed, axis=1, keepdims=True)
             normed = mixed * lax.rsqrt(mean + 1e-06) * gain_ref[...]
             att[h, i * tile : (i + 1) * tile] = normed.astype(att.dtype)
+        for b in range(2):
+            for d in range(1, n_tp):
+                att_copy(h, b, d).start()
         for d in range(1, n_tp):
-            att_copy(h, d).start()
-        gathered[h, :, pl.ds(pl.multiple_of(t * width, width), width)] = att[
-            h, pl.ds(pl.multiple_of(t * rows, rows), rows)
-        ]
-
-    def project(h):
-        for load in loads[h * n_tp : (h + 1) * n_tp]:
-            load.wait()
+
+            @pl.when(near(d))
+            def _():
+                att_copy(h, 2, d).start()
+
+        for b in range(3):
+            gathered[h, b, :, here] = att[h, block_rows(b, z, core)]
+
+    def await_rows(h, b):
         for d in range(1, n_tp):
-            att_copy(h, d).wait_recv()
+            if b < 2:
+                att_copy(h, b, d).wait_recv()
+            else:
+
+                @pl.when(near(n_tp - d))
+                def _():
+                    att_copy(h, b, d).wait_recv()
+
+        if b == 1:
+            relay_copy(h).start()
+        if b == 2:
+            relay_copy(h).wait_recv()
+
+    def project(h, b):
         return jnp.dot(
-            gathered[h],
-            weight[h][: n_tp * width],
-            preferred_element_type=jnp.float32,
-        )
-
-    absorb([[], [(0, 1), (0, 0)], [(0, 0), (0, 1), (1, 0)], [(1, 0), (2, 0), (1, 1), (0, 0)]], 1)
+            gathered[h, b], weight[h][: n_tp * width], preferred_element_type=jnp.float32
+        )
+
+    def normalize(base, projected):
+        new = (base.astype(jnp.float32) + projected).astype(jnp.bfloat16)
+        widened = new.astype(jnp.float32)
+        mean = jnp.mean(widened * widened, axis=1, keepdims=True)
+        return new, (widened * lax.rsqrt(mean + 1e-06) * norm_ref[...]).astype(jnp.bfloat16)
+
+    def far_rows(b):
+        await_rows(1, b)
+        if b == 2:
+            for part in range(2):
+                base_copy(2, part).wait_recv()
+        _, normed = normalize(bases[b - 1], parts[b] + project(1, b))
+        zrows[b - 1] = normed
+
+    absorb([[], [(0, 1), (0, 0)], [(0, 0), (0, 1), (1, 0)], [(1, 0), (2, 0), (1, 1), (0, 0)]], 1, True)
+
+    @pl.when(c == 0)
+    def _():
+        pass_base(1)
+
     finish(0)
     absorb([[], [], [(1, 1)], [(2, 1), (0, 1)]], 0)
 
@@ -790,17 +903,16 @@
             pl.semaphore_signal(go, inc=1, device_id=column(d), device_id_type=MESH)
 
     finish(1)
-    mine[...] = project(0)
-    new = (base_ref[...].astype(jnp.float32) + mine[...] + project(1)).astype(jnp.bfloat16)
+    for load in loads[: heads * n_tp]:
+        load.wait()
+    await_rows(0, 0)
+    parts[0] = project(0, 0)
+    await_rows(0, 1)
+    parts[1] = project(0, 1)
+    await_rows(1, 0)
+    new, normed = normalize(base_ref[...], parts[0] + project(1, 0))
     updated[...] = new
-    widened = new.astype(jnp.float32)
-    mean = jnp.mean(widened * widened, axis=1, keepdims=True)
-    x_ref[...] = (widened * lax.rsqrt(mean + 1e-06) * norm_ref[...]).astype(jnp.bfloat16)
-
-    def z_copy(d):
-        if d == 1:
-            return remote(x_ref, zrows.at[0], zs_send.at[1], zs_recv.at[1], far[1])
-        return remote(zrows.at[0], zrows.at[1], zs_send.at[2], zs_recv.at[2], twin)
+    x_ref[...] = normed
 
     def pack_copy(d, s):
         return remote(
@@ -833,11 +945,6 @@
         return remote(zsend.at[d - 1], zret.at[d - 1], zr_send.at[d], zr_recv.at[d], far[d])
 
     outer = (z == 0) | (z == n_z - 1)
-
-    @pl.when(jnp.logical_not(outer))
-    def _():
-        z_copy(1).start()
-
     for d in (1, 2):
         meta_copy(d).wait()
 
@@ -846,12 +953,6 @@
         return target == zmeta[s, r : r + 1, :rows]
 
     def pack_rows(s):
-        if s:
-            z_copy(s).wait_recv()
-        if s == 1:
-            z_copy(2).start()
-            for d in range(2, n_sp):
-                twin_copy(d).start()
         hits = route_hits(s, 0) | route_hits(s, 1)
         pick = jnp.where(hits, 1.0, 0.0).astype(jnp.bfloat16)
         source = x_ref[...] if s == 0 else zrows[s - 1]
@@ -863,11 +964,6 @@
         if s == 0:
             arrived[0, 0, 0] = packed[0]
             twin_copy(0).start()
-
-            @pl.when(outer)
-            def _():
-                z_copy(1).start()
-
         for d in range(1, n_sp):
             pack[s, d - 1] = packed[d]
             pack_copy(d, s).start()
@@ -879,10 +975,8 @@
         for d in range(n_sp):
             if s == TWIN:
                 twin_copy(d).wait_recv()
-            elif d:
+            elif s and d:
                 pack_copy(d, s).wait_recv()
-            if s == 0 and d == 1:
-                twin_copy(d).start()
             if s == TWIN or d:
                 share_copy(d, s).start()
         for d in range(n_sp):
@@ -920,7 +1014,14 @@
             total = total.astype(jnp.bfloat16)
             if s == TWIN:
                 own[s, d] = total
-                fold_copy(d).start()
+                if d in (1, 2):
+                    fold_copy(d).start()
+                else:
+
+                    @pl.when(jnp.logical_not(outer))
+                    def _():
+                        fold_copy(d).start()
+
             elif d == 0:
                 ret[s, 0] = total
             else:
@@ -952,9 +1053,16 @@
     pack_rows(0)
     for load in loads[heads * n_tp :]:
         load.wait()
+    far_rows(1)
+    pack_rows(1)
+    await_rows(0, 2)
+    parts[2] = project(0, 2)
+    for d in range(1, n_sp):
+        pack_copy(d, 0).wait_recv()
+        twin_copy(d).start()
+    far_rows(2)
+    pack_rows(2)
     run_experts(0)
-    pack_rows(1)
-    pack_rows(2)
     run_experts(1)
     reduce_pair(1)
     run_experts(TWIN)
@@ -962,14 +1070,20 @@
     run_experts(2)
     reduce_pair(2)
     mix_rows(1)
+
+    @pl.when(outer)
+    def _():
+        for d in (n_sp - 1, 0):
+            fold_copy(d).start()
+
     mix_rows(2)
     reduce_pair(0)
     merged = updated[...].astype(jnp.float32)
     for s in (1, 2):
         z_back(s).wait_recv()
         merged = merged + zret[s - 1].astype(jnp.float32)
-    mine[...] = merged
-    out_ref[...] = (mine[...] + mix_rows(0)).astype(jnp.bfloat16)
+    parts[0] = merged
+    out_ref[...] = (parts[0] + mix_rows(0)).astype(jnp.bfloat16)
 
     for k in range(n_sp):
         @pl.when(c == k)
@@ -977,11 +1091,20 @@
             for copy in first_sends[k] + late_sends[k]:
                 copy.wait_send()
 
-    for d in range(1, n_tp):
-        for h in range(heads):
-            att_copy(h, d).wait_send()
+    for h in range(heads):
+        for d in range(1, n_tp):
+            for b in range(2):
+                att_copy(h, b, d).wait_send()
+
+            @pl.when(near(d))
+            def _():
+                att_copy(h, 2, d).wait_send()
+
+        relay_copy(h).wait_send()
     for d in (1, 2):
-        z_copy(d).wait_send()
+        for side in range(2):
+            base_copy(d, side).wait_send()
+    for d in (1, 2):
         z_back(d).wait_send()
     for s in range(n_z):
         for d in range(n_sp):
@@ -995,22 +1118,14 @@
         fold_copy(d).wait_send()
 
 
-def masked_queries(queries, tile):
-    tokens, heads, pair = queries.shape
-    tiles = tokens // tile
-    first = (jnp.arange(pair) < pair // 2)[None, :]
-    q = jnp.transpose(queries, (1, 0, 2)).reshape(heads, tiles, 1, tile, pair)
-    sides = jnp.stack([first, ~first])
-    return jnp.where(sides, q, jnp.zeros((), q.dtype)).reshape(heads, tiles, 2 * tile, pair)
-
-
 def whole_layer(
     queries,
     key_pairs,
     head_values,
     lambdas,
     head_gain,
-    meta,
+    expert_ids,
+    route_weights,
     residual,
     norm_gain,
     out_weight,
@@ -1028,8 +1143,7 @@
     n_z = n_tp // CORES
     tile = math.gcd(tokens, 256)
     tiles = tokens // tile
-    q = masked_queries(queries, tile)
-    kv = jnp.transpose(jnp.stack([key_pairs, head_values]), (2, 0, 1, 3))
+    q, k, v = (jnp.transpose(x, (1, 0, 2)) for x in (queries, key_pairs, head_values))
     dma = pltpu.SemaphoreType.DMA
     vmem = pl.BlockSpec(memory_space=pltpu.VMEM)
     hbm = pl.BlockSpec(memory_space=pl.ANY)
@@ -1045,18 +1159,20 @@
     return pl.pallas_call(
         functools.partial(layer_kernel, n_sp, n_tp, (pair // 2) ** (-0.5)),
         out_shape=jax.ShapeDtypeStruct((rows, model), jnp.bfloat16),
-        in_specs=[pl.BlockSpec(memory_space=pltpu.SMEM)] + [vmem] * 6 + [hbm] * 4,
+        in_specs=[pl.BlockSpec(memory_space=pltpu.SMEM)] + [vmem] * 8 + [hbm] * 4,
         out_specs=vmem,
         scratch_shapes=[
-            buffer(heads, rows, n_tp * width),
-            buffer(n_sp - 1, *kv.shape),
+            buffer(heads, tiles, 2 * tile, pair),
+            buffer(heads, 3, rows, n_tp * width),
+            buffer(n_sp - 1, heads, 2, tokens, width),
             single(heads, tiles, 2 * tile, width),
             single(heads, tiles, 2 * tile, 1),
             single(heads, tiles, 2 * tile, 1),
             buffer(heads, tokens, width),
+            buffer(2, rows, model),
             buffer(rows, model),
             buffer(rows, model),
-            single(3, *meta.shape),
+            single(3, 8, rows + -rows % 128),
             buffer(*gate_weight.shape),
             buffer(*up_weight.shape),
             buffer(*down_weight.shape),
@@ -1070,16 +1186,18 @@
             buffer(2, rows, model),
             buffer(2, rows, model),
             buffer(n_sp, *block),
-            single(rows, model),
+            single(3, rows, model),
             dma((n_sp + 1, 2)),
             dma((n_sp - 1, heads, 2)),
-            dma((heads, n_tp)),
-            dma((heads, n_tp)),
+            dma((heads, 3, n_tp)),
+            dma((heads, 3, n_tp)),
+            dma((heads,)),
+            dma((heads,)),
+            dma((2, 2)),
+            dma((2, 2)),
             dma((n_z,)),
             dma((n_z,)),
             dma((heads * n_tp + 3,)),
-            dma((n_z,)),
-            dma((n_z,)),
             dma((n_sp, n_z)),
             dma((n_sp, n_z)),
             dma((n_sp, n_z)),
@@ -1103,9 +1221,11 @@
     )(
         lambdas,
         q,
-        kv,
+        k,
+        v,
         head_gain.reshape(1, -1),
-        meta,
+        expert_ids.T,
+        route_weights.T,
         residual,
         norm_gain.reshape(1, -1),
         out_weight.reshape(n_tp, heads, width, model),
@@ -1140,16 +1260,6 @@
     local_experts = gate_weight.shape[0]
     expert_count = local_experts * sp_count
     capacity = max(2, 4 * rows_here * route_count // (3 * expert_count))
-    flat_ids = expert_ids.reshape(-1)
-    indicator = (flat_ids[:, None] == jnp.arange(expert_count, dtype=jnp.int32)[None, :]).astype(
-        jnp.int32
-    )
-    ranking = jnp.sum(jnp.cumsum(indicator, axis=0) * indicator, axis=1) - 1
-    turned = (flat_ids - lax.axis_index("sp") * local_experts) % expert_count
-    near_slots = (turned * capacity + ranking).reshape(rows_here, route_count)
-    slots = flat_ids * capacity + ranking
-    meta = jnp.concatenate([near_slots.astype(jnp.float32), route_weights], axis=1).T
-    meta = jnp.pad(meta, ((0, 8 - 2 * route_count), (0, -rows_here % 128)), constant_values=-1.0)
     model_width = residual.shape[1]
     block_bytes = z_count * local_experts * capacity * model_width * 2
     if sp_count == PLANE and z_count == LAYERS and heads_here == HEADS_HERE and pair_width == value_width and (
@@ -1162,7 +1272,8 @@
             head_values,
             lambdas,
             head_gain,
-            meta,
+            expert_ids,
+            route_weights,
             residual,
             norm_gain,
             out_weight,
@@ -1173,6 +1284,16 @@
             tp_count,
             capacity,
         )
+    flat_ids = expert_ids.reshape(-1)
+    indicator = (flat_ids[:, None] == jnp.arange(expert_count, dtype=jnp.int32)[None, :]).astype(
+        jnp.int32
+    )
+    ranking = jnp.sum(jnp.cumsum(indicator, axis=0) * indicator, axis=1) - 1
+    turned = (flat_ids - lax.axis_index("sp") * local_experts) % expert_count
+    near_slots = (turned * capacity + ranking).reshape(rows_here, route_count)
+    slots = flat_ids * capacity + ranking
+    meta = jnp.concatenate([near_slots.astype(jnp.float32), route_weights], axis=1).T
+    meta = jnp.pad(meta, ((0, 8 - 2 * route_count), (0, -rows_here % 128)), constant_values=-1.0)
     updated, normed, zmeta = attend(
         queries,
         key_pairs,

time: 153 us -> 143 us (0.935)
  the two profiles are of different devices: /device:TPU:8 before, /device:TPU:0 now
where the time goes in v3:
time: 143 us; the launch traced here: 140 us
  Pallas kernels  134 us (94%)
  local copies, waits for them, and re-layouts  5.66 us (4%)
    pallas_call x1, Pallas kernels, whole_layer(): pl.pallas_call(functools.partial(layer_kernel, n_sp, n_tp, (pair // 2) **...  134 us
    unnamed x2, local copies, waits for them, and re-layouts  3.56 us

profile of v3, /device:TPU:0, one launch (start us, length us, event | category | flops | bytes accessed | tf_op | source)
XLA Modules:
  0.0 140.1 jit_solution(18283943474631303971)
XLA Ops:
  0.0 1.8 %copy.20 = bf16[768,2,128]{2,0,1:T(8,128)(2,1)} copy(bf16[768,2,128]{2,1,0:T(2,128)(2,1)} %param.13) | data formatting | bytes 786432 | tf_op args[0]
  1.8 2.1 %copy_bitcast_fusion = (bf16[2,768,128]{2,1,0:T(8,128)(2,1)}, bf16[2,768,128]{2,1,0:T(8,128)(2,1)}) fusion(bf16[768,2,128]{2,1,0:T(2,128)(2,1)} %param.15, bf16[768,2,128]{2,1,0:T(2,128)(2,1)} %param.14), kind=kLoop, calls=%fused_computation | loop fusion | bytes 1572864 | tf_op jit(solution)/shard_map/transpose | solution.py:1146
  3.9 134.5 %layer.1 = bf16[96,2048]{1,0:T(8,128)(2,1)} custom-call(f32[2]{0:T(128)} %lam_ref.1, bf16[2,768,128]{2,1,0:T(8,128)(2,1)} %bitcast.13, bf16[2,768,128]{2,1,0:T(8,128)(2,1)} %get-tuple-element.6.k_ref, bf16[2,768,128]{2,1,0:T(8,128)(2,1)} %get-tuple-element.5.v_ref, f32[1,128]{1,0:T(1,128)} %bitcast.17, s32[2,96]{1,0:T(2,128)} %bitcast.15, f32[2,96]{1,0:T(2,128)} %bitcast.16, ...), custom_call_target="tpu_custom_call" | custom-call | tf_op jit(solution)/shard_map/layer/pallas_call | solution.py:1159
  138.4 1.8 %copy.22 = bf16[96,2048]{1,0:T(8,128)(2,1)} copy(bf16[96,2048]{1,0:T(8,128)(2,1)} %layer.1) | data formatting | bytes 786432

commit v4 on v3

--- a/solution.py
+++ b/solution.py
@@ -530,7 +530,6 @@
     kvbuf,
     acc,
     top,
-    tot,
     att,
     bases,
     updated,
@@ -733,6 +732,9 @@
             * factor
         )
 
+    def with_ones(values):
+        return jnp.concatenate([values, jnp.ones_like(values)], axis=1)
+
     for i in range(tiles):
         extent = (i + 1) * tile
         for h in range(heads):
@@ -743,9 +745,10 @@
             high = jnp.max(s, axis=1, keepdims=True)
             p = jnp.exp2(s - high)
             top[h, i] = high
-            tot[h, i] = jnp.sum(p, axis=1, keepdims=True)
             acc[h, i] = jnp.dot(
-                p.astype(jnp.bfloat16), v_ref[h, :extent], preferred_element_type=jnp.float32
+                p.astype(jnp.bfloat16),
+                with_ones(v_ref[h, :extent]),
+                preferred_element_type=jnp.float32,
             )
 
     for k in range(n_sp):
@@ -782,7 +785,7 @@
                 def _():
                     pass_base(1)
 
-            keys, values = kvbuf[source, h, 0], kvbuf[source, h, 1]
+            keys, values = kvbuf[source, h, 0], with_ones(kvbuf[source, h, 1])
             results = []
             for i in range(tiles):
                 s = scores_of(h, i, keys)
@@ -790,13 +793,12 @@
                 high = jnp.maximum(before, jnp.max(s, axis=1, keepdims=True))
                 p = jnp.exp2(s - high)
                 decay = jnp.exp2(before - high)
-                total = tot[h, i] * decay + jnp.sum(p, axis=1, keepdims=True)
                 summed = acc[h, i] * decay + jnp.dot(
                     p.astype(jnp.bfloat16), values, preferred_element_type=jnp.float32
                 )
-                results.append((high, total, summed))
+                results.append((high, summed))
             for i in range(tiles):
-                top[h, i], tot[h, i], acc[h, i] = results[i]
+                top[h, i], acc[h, i] = results[i]
             return code // 8
 
         lax.fori_loop(0, count, piece_step, code)
@@ -837,22 +839,27 @@
 
     def finish(h):
         for i in range(tiles):
-            both = acc[h, i] / tot[h, i]
+            both = acc[h, i, :, :width] / acc[h, i, :, width:]
             mixed = both[:tile] - lam_ref[h] * both[tile:]
             mean = jnp.mean(mixed * mixed, axis=1, keepdims=True)
             normed = mixed * lax.rsqrt(mean + 1e-06) * gain_ref[...]
             att[h, i * tile : (i + 1) * tile] = normed.astype(att.dtype)
-        for b in range(2):
-            for d in range(1, n_tp):
-                att_copy(h, b, d).start()
         for d in range(1, n_tp):
-
-            @pl.when(near(d))
-            def _():
-                att_copy(h, 2, d).start()
-
+            att_copy(h, 0, d).start()
         for b in range(3):
             gathered[h, b, :, here] = att[h, block_rows(b, z, core)]
+
+    def finish_far():
+        for h in range(heads):
+            for d in range(1, n_tp):
+                att_copy(h, 1, d).start()
+        for h in range(heads):
+            for d in range(1, n_tp):
+
+                @pl.when(near(d))
+                def _():
+                    att_copy(h, 2, d).start()
+
 
     def await_rows(h, b):
         for d in range(1, n_tp):
@@ -881,6 +888,8 @@
         return new, (widened * lax.rsqrt(mean + 1e-06) * norm_ref[...]).astype(jnp.bfloat16)
 
     def far_rows(b):
+        await_rows(0, b)
+        parts[b] = project(0, b)
         await_rows(1, b)
         if b == 2:
             for part in range(2):
@@ -903,12 +912,11 @@
             pl.semaphore_signal(go, inc=1, device_id=column(d), device_id_type=MESH)
 
     finish(1)
+    finish_far()
     for load in loads[: heads * n_tp]:
         load.wait()
     await_rows(0, 0)
     parts[0] = project(0, 0)
-    await_rows(0, 1)
-    parts[1] = project(0, 1)
     await_rows(1, 0)
     new, normed = normalize(base_ref[...], parts[0] + project(1, 0))
     updated[...] = new
@@ -936,13 +944,38 @@
     def fold_copy(d):
         return remote(own.at[TWIN, d], fold.at[d], fo_send.at[d], fo_recv.at[d], twin)
 
-    def back_copy(d, s):
+    def columns_of(part):
+        return slice(part * (model // 2), (part + 1) * (model // 2))
+
+    def back_copy(d, s, part):
         return remote(
-            own.at[s, d], ret.at[s, d], rt_send.at[d, s], rt_recv.at[d, s], column(n_sp - d)
-        )
-
-    def z_back(d):
-        return remote(zsend.at[d - 1], zret.at[d - 1], zr_send.at[d], zr_recv.at[d], far[d])
+            own.at[s, d, :, :, columns_of(part)],
+            ret.at[s, d, :, :, columns_of(part)],
+            rt_send.at[d, s, part],
+            rt_recv.at[d, s, part],
+            column(n_sp - d),
+        )
+
+    def z_part(d, part, target):
+        return remote(
+            zsend.at[d - 1, :, columns_of(part)],
+            zret.at[d - 1, :, columns_of(part)],
+            zr_send.at[d, part],
+            zr_recv.at[d, part],
+            target,
+        )
+
+    def z_back(d, part):
+        return z_part(d, part, far[d])
+
+    def z_join(part):
+        return remote(
+            zsend.at[0, :, columns_of(part)],
+            zret.at[0, :, columns_of(part)],
+            zr_send.at[0, part],
+            zr_recv.at[0, part],
+            twin,
+        )
 
     outer = (z == 0) | (z == n_z - 1)
     for d in (1, 2):
@@ -1026,24 +1059,48 @@
                 ret[s, 0] = total
             else:
                 own[s, d] = total
-                back_copy(d, s).start()
-
-    def mix_rows(s):
+                back_copy(d, s, 0).start()
+                if s == 0:
+                    back_copy(d, s, 1).start()
+        if s in (1, 2):
+            for d in range(1, n_sp):
+                back_copy(d, s, 1).start()
+
+    def mix_rows(s, part):
         for d in range(1, n_sp):
-            back_copy(d, s).wait_recv()
+            back_copy(d, s, part).wait_recv()
+        columns = columns_of(part)
         mixing = jnp.where(route_hits(s, 0), zmeta[s, 2:3, :rows], 0.0) + jnp.where(
             route_hits(s, 1), zmeta[s, 3:4, :rows], 0.0
         )
         high = mixing.astype(jnp.bfloat16)
         low = (mixing - high.astype(jnp.float32)).astype(jnp.bfloat16)
-        back = ret[s].reshape(slots, model)
+        back = ret[s, :, :, :, columns].reshape(slots, model // 2)
         numbers = (((0,), (0,)), ((), ()))
         merged = lax.dot_general(
             high, back, numbers, preferred_element_type=jnp.float32
         ) + lax.dot_general(low, back, numbers, preferred_element_type=jnp.float32)
-        if s:
-            zsend[s - 1] = merged.astype(jnp.bfloat16)
-            z_back(s).start()
+        if s == 1:
+            zsend[0, :, columns] = merged.astype(jnp.bfloat16)
+
+            @pl.when(outer)
+            def _():
+                z_join(part).start()
+
+            @pl.when(jnp.logical_not(outer))
+            def _():
+                z_back(1, part).start()
+
+        if s == 2:
+            parts[0, :, columns] = merged
+
+            @pl.when(jnp.logical_not(outer))
+            def _():
+                z_join(part).wait_recv()
+                parts[0, :, columns] = parts[0, :, columns] + zret[0, :, columns].astype(jnp.float32)
+
+            zsend[1, :, columns] = parts[0, :, columns].astype(jnp.bfloat16)
+            z_back(2, part).start()
         return merged
 
     @pl.when(c != n_sp - 1)
@@ -1055,8 +1112,6 @@
         load.wait()
     far_rows(1)
     pack_rows(1)
-    await_rows(0, 2)
-    parts[2] = project(0, 2)
     for d in range(1, n_sp):
         pack_copy(d, 0).wait_recv()
         twin_copy(d).start()
@@ -1069,21 +1124,31 @@
     reduce_pair(TWIN)
     run_experts(2)
     reduce_pair(2)
-    mix_rows(1)
+    mix_rows(1, 0)
+    mix_rows(1, 1)
 
     @pl.when(outer)
     def _():
         for d in (n_sp - 1, 0):
             fold_copy(d).start()
 
-    mix_rows(2)
+    mix_rows(2, 0)
+    mix_rows(2, 1)
     reduce_pair(0)
-    merged = updated[...].astype(jnp.float32)
-    for s in (1, 2):
-        z_back(s).wait_recv()
-        merged = merged + zret[s - 1].astype(jnp.float32)
-    parts[0] = merged
-    out_ref[...] = (parts[0] + mix_rows(0)).astype(jnp.bfloat16)
+    parts[0] = updated[...].astype(jnp.float32)
+    for part in range(2):
+        columns = columns_of(part)
+
+        @pl.when(outer)
+        def _():
+            z_back(1, part).wait_recv()
+            parts[0, :, columns] = parts[0, :, columns] + zret[0, :, columns].astype(jnp.float32)
+
+        z_back(2, part).wait_recv()
+        parts[0, :, columns] = parts[0, :, columns] + zret[1, :, columns].astype(jnp.float32)
+    for part in range(2):
+        columns = columns_of(part)
+        out_ref[:, columns] = (parts[0, :, columns] + mix_rows(0, part)).astype(jnp.bfloat16)
 
     for k in range(n_sp):
         @pl.when(c == k)
@@ -1104,13 +1169,23 @@
     for d in (1, 2):
         for side in range(2):
             base_copy(d, side).wait_send()
-    for d in (1, 2):
-        z_back(d).wait_send()
+    for part in range(2):
+
+        @pl.when(outer)
+        def _():
+            z_join(part).wait_send()
+
+        @pl.when(jnp.logical_not(outer))
+        def _():
+            z_back(1, part).wait_send()
+
+        z_back(2, part).wait_send()
     for s in range(n_z):
         for d in range(n_sp):
             if d and s != TWIN:
                 pack_copy(d, s).wait_send()
-                back_copy(d, s).wait_send()
+                for part in range(2):
+                    back_copy(d, s, part).wait_send()
             share_copy(d, s).wait_send()
         pair_copy(s).wait_send()
     for d in range(n_sp):
@@ -1165,8 +1240,7 @@
             buffer(heads, tiles, 2 * tile, pair),
             buffer(heads, 3, rows, n_tp * width),
             buffer(n_sp - 1, heads, 2, tokens, width),
-            single(heads, tiles, 2 * tile, width),
-            single(heads, tiles, 2 * tile, 1),
+            single(heads, tiles, 2 * tile, 2 * width),
             single(heads, tiles, 2 * tile, 1),
             buffer(heads, tokens, width),
             buffer(2, rows, model),
@@ -1204,10 +1278,10 @@
             dma((n_sp, n_z)),
             dma((n_z,)),
             dma((n_z,)),
-            dma((n_sp, n_z)),
-            dma((n_sp, n_z)),
-            dma((n_z,)),
-            dma((n_z,)),
+            dma((n_sp, n_z, 2)),
+            dma((n_sp, n_z, 2)),
+            dma((n_z, 2)),
+            dma((n_z, 2)),
             dma((n_sp,)),
             dma((n_sp,)),
             dma((n_sp,)),

time: 143 us -> 138 us (0.965)
  Pallas kernels: 134 us -> 131 us
    pallas_call x1, Pallas kernels: 134 us -> 131 us  [whole_layer(): pl.pallas_call(functools.partial(layer_kernel, n_sp, n_tp, (pair // 2) **...]
where the time goes in v4:
time: 138 us; the launch traced here: 136 us
  Pallas kernels  131 us (95%)
  local copies, waits for them, and re-layouts  5.66 us (4%)
    pallas_call x1, Pallas kernels, whole_layer(): pl.pallas_call(functools.partial(layer_kernel, n_sp, n_tp, (pair // 2) **...  131 us
    unnamed x2, local copies, waits for them, and re-layouts  3.56 us

profile of v4, /device:TPU:0, one launch (start us, length us, event | category | flops | bytes accessed | tf_op | source)
XLA Modules:
  0.0 136.4 jit_solution(11621704683908215516)
XLA Ops:
  0.0 1.8 %copy.20 = bf16[768,2,128]{2,0,1:T(8,128)(2,1)} copy(bf16[768,2,128]{2,1,0:T(2,128)(2,1)} %param.13) | data formatting | bytes 786432 | tf_op args[0]
  1.8 2.1 %copy_bitcast_fusion = (bf16[2,768,128]{2,1,0:T(8,128)(2,1)}, bf16[2,768,128]{2,1,0:T(8,128)(2,1)}) fusion(bf16[768,2,128]{2,1,0:T(2,128)(2,1)} %param.15, bf16[768,2,128]{2,1,0:T(2,128)(2,1)} %param.14), kind=kLoop, calls=%fused_computation | loop fusion | bytes 1572864 | tf_op jit(solution)/shard_map/transpose | solution.py:1221
  3.9 130.8 %layer.1 = bf16[96,2048]{1,0:T(8,128)(2,1)} custom-call(f32[2]{0:T(128)} %lam_ref.1, bf16[2,768,128]{2,1,0:T(8,128)(2,1)} %bitcast.13, bf16[2,768,128]{2,1,0:T(8,128)(2,1)} %get-tuple-element.6.k_ref, bf16[2,768,128]{2,1,0:T(8,128)(2,1)} %get-tuple-element.5.v_ref, f32[1,128]{1,0:T(1,128)} %bitcast.17, s32[2,96]{1,0:T(2,128)} %bitcast.15, f32[2,96]{1,0:T(2,128)} %bitcast.16, ...), custom_call_target="tpu_custom_call" | custom-call | tf_op jit(solution)/shard_map/layer/pallas_call | solution.py:1234
  134.7 1.8 %copy.22 = bf16[96,2048]{1,0:T(8,128)(2,1)} copy(bf16[96,2048]{1,0:T(8,128)(2,1)} %layer.1) | data formatting | bytes 786432

commit v5 on v4

--- a/solution.py
+++ b/solution.py
@@ -512,9 +512,9 @@
     n_tp,
     scale,
     lam_ref,
-    raw_ref,
-    k_ref,
-    v_ref,
+    raw_q,
+    raw_k,
+    raw_v,
     gain_ref,
     ids_ref,
     mix_ref,
@@ -526,6 +526,8 @@
     down_hbm,
     out_ref,
     q_ref,
+    k_ref,
+    v_ref,
     gathered,
     kvbuf,
     acc,
@@ -617,6 +619,9 @@
         pl.semaphore_signal(barrier, inc=1, device_id=column(d), device_id_type=MESH)
     for d in range(1, n_tp):
         pl.semaphore_signal(barrier, inc=1, device_id=(c, (t + d) % n_tp), device_id_type=MESH)
+    for h in range(heads):
+        k_ref[h] = raw_k[:, h, :]
+        v_ref[h] = raw_v[:, h, :]
     pl.semaphore_wait(barrier, n_sp + n_tp - 2)
 
     def remote(src, dst, send, recv, target):
@@ -715,10 +720,11 @@
     for d in (1, 2):
         meta_copy(d).start()
 
-    side = lax.broadcasted_iota(jnp.int32, (tile, raw_ref.shape[2]), 1) < raw_ref.shape[2] // 2
+    side = lax.broadcasted_iota(jnp.int32, (tile, raw_q.shape[2]), 1) < raw_q.shape[2] // 2
     for h in range(heads):
+        att[h] = raw_q[:, h, :]
         for i in range(tiles):
-            part = raw_ref[h, i * tile : (i + 1) * tile]
+            part = att[h, i * tile : (i + 1) * tile]
             q_ref[h, i, :tile] = jnp.where(side, part, jnp.zeros_like(part))
             q_ref[h, i, tile:] = jnp.where(side, jnp.zeros_like(part), part)
 
@@ -1103,6 +1109,40 @@
             z_back(2, part).start()
         return merged
 
+    def sent_early():
+        for k in range(n_sp):
+            @pl.when(c == k)
+            def _():
+                for copy in first_sends[k] + late_sends[k]:
+                    copy.wait_send()
+
+        for h in range(heads):
+            for d in range(1, n_tp):
+                for b in range(2):
+                    att_copy(h, b, d).wait_send()
+
+                @pl.when(near(d))
+                def _():
+                    att_copy(h, 2, d).wait_send()
+
+            relay_copy(h).wait_send()
+        for d in (1, 2):
+            for side in range(2):
+                base_copy(d, side).wait_send()
+
+    def sent_later():
+        for s in range(n_z):
+            for d in range(n_sp):
+                if d and s != TWIN:
+                    pack_copy(d, s).wait_send()
+                if d and s in (1, 2):
+                    for part in range(2):
+                        back_copy(d, s, part).wait_send()
+                share_copy(d, s).wait_send()
+            pair_copy(s).wait_send()
+        for d in range(n_sp):
+            twin_copy(d).wait_send()
+
     @pl.when(c != n_sp - 1)
     def _():
         pl.semaphore_wait(go, 1)
@@ -1118,6 +1158,7 @@
     far_rows(2)
     pack_rows(2)
     run_experts(0)
+    sent_early()
     run_experts(1)
     reduce_pair(1)
     run_experts(TWIN)
@@ -1134,6 +1175,7 @@
 
     mix_rows(2, 0)
     mix_rows(2, 1)
+    sent_later()
     reduce_pair(0)
     parts[0] = updated[...].astype(jnp.float32)
     for part in range(2):
@@ -1150,25 +1192,6 @@
         columns = columns_of(part)
         out_ref[:, columns] = (parts[0, :, columns] + mix_rows(0, part)).astype(jnp.bfloat16)
 
-    for k in range(n_sp):
-        @pl.when(c == k)
-        def _():
-            for copy in first_sends[k] + late_sends[k]:
-                copy.wait_send()
-
-    for h in range(heads):
-        for d in range(1, n_tp):
-            for b in range(2):
-                att_copy(h, b, d).wait_send()
-
-            @pl.when(near(d))
-            def _():
-                att_copy(h, 2, d).wait_send()
-
-        relay_copy(h).wait_send()
-    for d in (1, 2):
-        for side in range(2):
-            base_copy(d, side).wait_send()
     for part in range(2):
 
         @pl.when(outer)
@@ -1180,17 +1203,11 @@
             z_back(1, part).wait_send()
 
         z_back(2, part).wait_send()
-    for s in range(n_z):
-        for d in range(n_sp):
-            if d and s != TWIN:
-                pack_copy(d, s).wait_send()
-                for part in range(2):
-                    back_copy(d, s, part).wait_send()
-            share_copy(d, s).wait_send()
-        pair_copy(s).wait_send()
     for d in range(n_sp):
-        twin_copy(d).wait_send()
         fold_copy(d).wait_send()
+        if d:
+            for part in range(2):
+                back_copy(d, 0, part).wait_send()
 
 
 def whole_layer(
@@ -1218,7 +1235,6 @@
     n_z = n_tp // CORES
     tile = math.gcd(tokens, 256)
     tiles = tokens // tile
-    q, k, v = (jnp.transpose(x, (1, 0, 2)) for x in (queries, key_pairs, head_values))
     dma = pltpu.SemaphoreType.DMA
     vmem = pl.BlockSpec(memory_space=pltpu.VMEM)
     hbm = pl.BlockSpec(memory_space=pl.ANY)
@@ -1238,6 +1254,8 @@
         out_specs=vmem,
         scratch_shapes=[
             buffer(heads, tiles, 2 * tile, pair),
+            buffer(heads, tokens, pair),
+            buffer(heads, tokens, width),
             buffer(heads, 3, rows, n_tp * width),
             buffer(n_sp - 1, heads, 2, tokens, width),
             single(heads, tiles, 2 * tile, 2 * width),
@@ -1294,9 +1312,9 @@
         name="layer",
     )(
         lambdas,
-        q,
-        k,
-        v,
+        queries,
+        key_pairs,
+        head_values,
         head_gain.reshape(1, -1),
         expert_ids.T,
         route_weights.T,

time: 138 us -> 134 us (0.971)
  local copies, waits for them, and re-layouts: 5.66 us -> 1.77 us
    transpose x1 -> x0, local copies, waits for them, and re-layouts: 2.1 us -> none  [whole_layer(): jnp.transpose(x, (1, 0, 2))]
    unnamed x2 -> x1, local copies, waits for them, and re-layouts: 3.56 us -> 1.77 us
where the time goes in v5:
time: 134 us; the launch traced here: 132 us
  Pallas kernels  131 us (98%)
  local copies, waits for them, and re-layouts  1.77 us (1%)
    pallas_call x1, Pallas kernels, whole_layer(): pl.pallas_call(functools.partial(layer_kernel, n_sp, n_tp, (pair // 2) **...  131 us

profile of v5, /device:TPU:0, one launch (start us, length us, event | category | flops | bytes accessed | tf_op | source)
XLA Modules:
  0.0 132.4 jit_solution(854259578468027213)
XLA Ops:
  0.0 130.6 %layer.1 = bf16[96,2048]{1,0:T(8,128)(2,1)} custom-call(f32[2]{0:T(128)} %lam_ref.1, bf16[768,2,128]{2,1,0:T(2,128)(2,1)} %raw_q.1, bf16[768,2,128]{2,1,0:T(2,128)(2,1)} %raw_k.1, bf16[768,2,128]{2,1,0:T(2,128)(2,1)} %raw_v.1, f32[1,128]{1,0:T(1,128)} %bitcast.9, s32[2,96]{1,0:T(2,128)} %bitcast.7, f32[2,96]{1,0:T(2,128)} %bitcast.8, ...), custom_call_target="tpu_custom_call" | custom-call | tf_op jit(solution)/shard_map/layer/pallas_call | solution.py:1250
  130.6 1.8 %copy.15 = bf16[96,2048]{1,0:T(8,128)(2,1)} copy(bf16[96,2048]{1,0:T(8,128)(2,1)} %layer.1) | data formatting | bytes 786432

commit v6 on v5

--- a/solution.py
+++ b/solution.py
@@ -598,7 +598,13 @@
     twin_z = z + 1 - 2 * (z % 2)
     far_z = (z + n_z // 2) % n_z
     twin = (c, twin_z * CORES + core)
-    far = [None, (c, far_z * CORES + core), (c, (far_z + 1 - 2 * (far_z % 2)) * CORES + core)]
+    far = [
+        None,
+        (c, far_z * CORES + core),
+        (c, (far_z + 1 - 2 * (far_z % 2)) * CORES + core),
+        twin,
+    ]
+    split = fold.shape[3]
 
     weight = (psend, precv)
     loads = [
@@ -717,7 +723,7 @@
         rank = jnp.sum(jnp.where(named[r], ranks, 0.0), axis=0, keepdims=True)
         zmeta[0, r : r + 1, :rows] = (turned * cap).astype(jnp.float32) + rank
         zmeta[0, 2 + r : 3 + r, :rows] = mix_ref[r : r + 1, :]
-    for d in (1, 2):
+    for d in (1, 2, TWIN):
         meta_copy(d).start()
 
     side = lax.broadcasted_iota(jnp.int32, (tile, raw_q.shape[2]), 1) < raw_q.shape[2] // 2
@@ -948,9 +954,13 @@
         return remote(psend.at[block], precv.at[block], pp_send.at[s], pp_recv.at[s], partner)
 
     def fold_copy(d):
-        return remote(own.at[TWIN, d], fold.at[d], fo_send.at[d], fo_recv.at[d], twin)
+        return remote(
+            own.at[TWIN, d, :, :, :split], fold.at[d], fo_send.at[d], fo_recv.at[d], twin
+        )
 
     def columns_of(part):
+        if part == 2:
+            return slice(split, model)
         return slice(part * (model // 2), (part + 1) * (model // 2))
 
     def back_copy(d, s, part):
@@ -984,7 +994,7 @@
         )
 
     outer = (z == 0) | (z == n_z - 1)
-    for d in (1, 2):
+    for d in (1, 2, TWIN):
         meta_copy(d).wait()
 
     def route_hits(s, r):
@@ -1049,7 +1059,9 @@
             )
             if s == 0:
                 fold_copy(d).wait_recv()
-                total = total + fold[d].astype(jnp.float32)
+                total = jnp.concatenate(
+                    [total[:, :, :split] + fold[d].astype(jnp.float32), total[:, :, split:]], axis=2
+                )
             total = total.astype(jnp.bfloat16)
             if s == TWIN:
                 own[s, d] = total
@@ -1061,6 +1073,10 @@
                     def _():
                         fold_copy(d).start()
 
+                if d:
+                    back_copy(d, TWIN, 2).start()
+                else:
+                    ret[TWIN, 0, :, :, split:] = total[:, :, split:]
             elif d == 0:
                 ret[s, 0] = total
             else:
@@ -1081,7 +1097,7 @@
         )
         high = mixing.astype(jnp.bfloat16)
         low = (mixing - high.astype(jnp.float32)).astype(jnp.bfloat16)
-        back = ret[s, :, :, :, columns].reshape(slots, model // 2)
+        back = ret[s, :, :, :, columns].reshape(slots, -1)
         numbers = (((0,), (0,)), ((), ()))
         merged = lax.dot_general(
             high, back, numbers, preferred_element_type=jnp.float32
@@ -1097,6 +1113,9 @@
             def _():
                 z_back(1, part).start()
 
+        if s == TWIN:
+            zsend[TWIN - 1, :, columns] = merged.astype(jnp.bfloat16)
+            z_back(TWIN, 2).start()
         if s == 2:
             parts[0, :, columns] = merged
 
@@ -1138,6 +1157,8 @@
                 if d and s in (1, 2):
                     for part in range(2):
                         back_copy(d, s, part).wait_send()
+                if d and s == TWIN:
+                    back_copy(d, s, 2).wait_send()
                 share_copy(d, s).wait_send()
             pair_copy(s).wait_send()
         for d in range(n_sp):
@@ -1173,6 +1194,7 @@
         for d in (n_sp - 1, 0):
             fold_copy(d).start()
 
+    mix_rows(TWIN, 2)
     mix_rows(2, 0)
     mix_rows(2, 1)
     sent_later()
@@ -1188,6 +1210,8 @@
 
         z_back(2, part).wait_recv()
         parts[0, :, columns] = parts[0, :, columns] + zret[1, :, columns].astype(jnp.float32)
+    z_back(TWIN, 2).wait_recv()
+    parts[0, :, split:] = parts[0, :, split:] + zret[TWIN - 1, :, split:].astype(jnp.float32)
     for part in range(2):
         columns = columns_of(part)
         out_ref[:, columns] = (parts[0, :, columns] + mix_rows(0, part)).astype(jnp.bfloat16)
@@ -1203,6 +1227,7 @@
             z_back(1, part).wait_send()
 
         z_back(2, part).wait_send()
+    z_back(TWIN, 2).wait_send()
     for d in range(n_sp):
         fold_copy(d).wait_send()
         if d:
@@ -1264,7 +1289,7 @@
             buffer(2, rows, model),
             buffer(rows, model),
             buffer(rows, model),
-            single(3, 8, rows + -rows % 128),
+            single(4, 8, rows + -rows % 128),
             buffer(*gate_weight.shape),
             buffer(*up_weight.shape),
             buffer(*down_weight.shape),
@@ -1274,10 +1299,10 @@
             buffer(flat, model),
             buffer(n_z, n_sp, *block),
             buffer(flat, model),
-            buffer(3, n_sp, *block),
-            buffer(2, rows, model),
-            buffer(2, rows, model),
-            buffer(n_sp, *block),
+            buffer(n_z, n_sp, *block),
+            buffer(3, rows, model),
+            buffer(3, rows, model),
+            buffer(n_sp, local, cap, model - model // 4),
             single(3, rows, model),
             dma((n_sp + 1, 2)),
             dma((n_sp - 1, heads, 2)),
@@ -1296,10 +1321,10 @@
             dma((n_sp, n_z)),
             dma((n_z,)),
             dma((n_z,)),
-            dma((n_sp, n_z, 2)),
-            dma((n_sp, n_z, 2)),
-            dma((n_z, 2)),
-            dma((n_z, 2)),
+            dma((n_sp, n_z, 3)),
+            dma((n_sp, n_z, 3)),
+            dma((n_z, 3)),
+            dma((n_z, 3)),
             dma((n_sp,)),
             dma((n_sp,)),
             dma((n_sp,)),

time: 134 us -> 131 us (0.978)
  Pallas kernels: 131 us -> 128 us
    pallas_call x1, Pallas kernels: 131 us -> 128 us  [whole_layer(): pl.pallas_call(functools.partial(layer_kernel, n_sp, n_tp, (pair // 2) **...]
where the time goes in v6:
time: 131 us; the launch traced here: 130 us
  Pallas kernels  128 us (98%)
  local copies, waits for them, and re-layouts  1.77 us (1%)
    pallas_call x1, Pallas kernels, whole_layer(): pl.pallas_call(functools.partial(layer_kernel, n_sp, n_tp, (pair // 2) **...  128 us

profile of v6, /device:TPU:0, one launch (start us, length us, event | category | flops | bytes accessed | tf_op | source)
XLA Modules:
  0.0 129.6 jit_solution(1762373601471917930)
XLA Ops:
  0.0 127.8 %layer.1 = bf16[96,2048]{1,0:T(8,128)(2,1)} custom-call(f32[2]{0:T(128)} %lam_ref.1, bf16[768,2,128]{2,1,0:T(2,128)(2,1)} %raw_q.1, bf16[768,2,128]{2,1,0:T(2,128)(2,1)} %raw_k.1, bf16[768,2,128]{2,1,0:T(2,128)(2,1)} %raw_v.1, f32[1,128]{1,0:T(1,128)} %bitcast.9, s32[2,96]{1,0:T(2,128)} %bitcast.7, f32[2,96]{1,0:T(2,128)} %bitcast.8, ...), custom_call_target="tpu_custom_call" | custom-call | tf_op jit(solution)/shard_map/layer/pallas_call | solution.py:1275
  127.9 1.8 %copy.15 = bf16[96,2048]{1,0:T(8,128)(2,1)} copy(bf16[96,2048]{1,0:T(8,128)(2,1)} %layer.1) | data formatting | bytes 786432

commit v7 on v6

--- a/solution.py
+++ b/solution.py
@@ -1065,7 +1065,7 @@
             total = total.astype(jnp.bfloat16)
             if s == TWIN:
                 own[s, d] = total
-                if d in (1, 2):
+                if d:
                     fold_copy(d).start()
                 else:
 
@@ -1191,8 +1191,7 @@
 
     @pl.when(outer)
     def _():
-        for d in (n_sp - 1, 0):
-            fold_copy(d).start()
+        fold_copy(0).start()
 
     mix_rows(TWIN, 2)
     mix_rows(2, 0)

time: 131 us -> 131 us (level)
  no operation moved by 1% of the time
where the time goes in v7:
time: 131 us; the launch traced here: 129 us
  Pallas kernels  128 us (98%)
  local copies, waits for them, and re-layouts  1.77 us (1%)
    pallas_call x1, Pallas kernels, whole_layer(): pl.pallas_call(functools.partial(layer_kernel, n_sp, n_tp, (pair // 2) **...  128 us

profile of v7, /device:TPU:0, one launch (start us, length us, event | category | flops | bytes accessed | tf_op | source)
XLA Modules:
  0.0 129.3 jit_solution(5276320151703506945)
XLA Ops:
  0.0 127.5 %layer.1 = bf16[96,2048]{1,0:T(8,128)(2,1)} custom-call(f32[2]{0:T(128)} %lam_ref.1, bf16[768,2,128]{2,1,0:T(2,128)(2,1)} %raw_q.1, bf16[768,2,128]{2,1,0:T(2,128)(2,1)} %raw_k.1, bf16[768,2,128]{2,1,0:T(2,128)(2,1)} %raw_v.1, f32[1,128]{1,0:T(1,128)} %bitcast.9, s32[2,96]{1,0:T(2,128)} %bitcast.7, f32[2,96]{1,0:T(2,128)} %bitcast.8, ...), custom_call_target="tpu_custom_call" | custom-call | tf_op jit(solution)/shard_map/layer/pallas_call | solution.py:1274
  127.5 1.8 %copy.15 = bf16[96,2048]{1,0:T(8,128)(2,1)} copy(bf16[96,2048]{1,0:T(8,128)(2,1)} %layer.1) | data formatting | bytes 786432
